TPU v7x, 512 devices: a whole 4x4x16 slice. The times are simulated.
512 devices in a mesh: fs: 64 (over z, y), tp: 8 (over x, core).
Axes of the slice: x: 4, y: 4, z: 16, core: 2. Of those that a mesh axis runs over, the one named last changes fastest.
Arguments:
- normed_input: bfloat16 [32768, 4096], P('fs', 'tp'), may hold values from -16 to 16
- value_cotangent: bfloat16 [32768, 2048], P('fs', 'tp'), may hold values from -0.005859375 to 0.005859375
- mixer_output: bfloat16 [32768, 2048], P('fs', 'tp'), may hold values from -6 to 6
- output_cotangent: bfloat16 [32768, 4096], P('fs', 'tp'), may hold values from -0.0078125 to 0.0078125
- value_factor: bfloat16 [4096, 128], replicated, may hold values from -0.5 to 0.5
- output_factor: bfloat16 [2048, 128], replicated, may hold values from -0.5 to 0.5
- value_master: float32 [4096, 2048], P('fs', 'tp'), may hold values from -0.09375 to 0.09375
- value_moment: float32 [128, 2048], P(None, 'tp'), may hold values from -6 to 6
- value_second: float32 [128, 2048], P(None, 'tp'), may hold values from 0.0625 to 16, as said below
- output_master: float32 [2048, 4096], P('fs', 'tp'), may hold values from -0.125 to 0.125
- output_moment: float32 [128, 4096], P(None, 'tp'), may hold values from -6 to 6
- output_second: float32 [128, 4096], P(None, 'tp'), may hold values from 0.0625 to 16, as said below
Outputs:
- value_step: float32 [4096, 2048], P('fs', 'tp')
- value_new: float32 [4096, 2048], P('fs', 'tp')
- value_copy: bfloat16 [4096, 2048], P(None, 'tp')
- value_moment_new: float32 [128, 2048], P(None, 'tp')
- value_second_new: float32 [128, 2048], P(None, 'tp')
- output_step: float32 [2048, 4096], P('fs', 'tp')
- output_new: float32 [2048, 4096], P('fs', 'tp')
- output_copy: bfloat16 [2048, 4096], P(None, 'tp')
- output_moment_new: float32 [128, 4096], P(None, 'tp')
- output_second_new: float32 [128, 4096], P(None, 'tp')
Inputs may be any that keep to these rules, and one draw needn't show every extreme that they name: `value_second`: positive, with a scale that differs between groups of columns. `output_second`: positive, with a scale that differs between groups of columns.
All inputs are finite; a program needn't handle non-finite values.
Results may differ from a plain program's by a relative error of at most 0.004.
Values may be sent and summed in bfloat16 or wider, within the bound.
A program may use at most 64 MiB of HBM per device.

v0:
```python
import jax
import jax.numpy as jnp
from jax import lax
from jax.sharding import Mesh
from jax.sharding import PartitionSpec as P

D = 4096
WIDTH = 2048
R = 128
FS = ("fs_0", "fs_1")


BETA_ONE = 0.8
BETA_TWO = 0.9
EPSILON = 1e-08
STEP_RATE = 0.005
FLOOR = 0.25


def sent_to_all(shard, axis):
    copies = jnp.broadcast_to(shard, (lax.axis_size(axis), *shard.shape))
    return lax.all_to_all(copies, axis, split_axis=0, concat_axis=0, tiled=True)


def taken_together(shard, axis):
    return sent_to_all(shard, axis).astype(jnp.float32).sum(axis=0)


def padded_to(lines, size):
    spare = -lines.shape[0] % size
    if not spare:
        return lines
    return jnp.concatenate([lines, jnp.zeros((spare, *lines.shape[1:]), lines.dtype)])


def own_block(parts, axes, sequence):
    inside = parts.shape[1:]
    parts = parts.reshape(*(lax.axis_size(a) for a in axes), *inside)
    parts = jnp.moveaxis(parts, sequence, range(len(axes))).reshape(-1, *inside)
    for k in sequence:
        parts = lax.psum_scatter(parts, axes[k], scatter_dimension=0, tiled=True)
    return parts[0]


def stacked_from(shard, axes, sequence):
    parts = shard
    for k in sequence:
        parts = lax.all_gather(parts, axes[k])
    done = sequence[::-1]
    back = [done.index(k) for k in range(len(axes))]
    parts = parts.transpose(*back, *range(len(axes), parts.ndim))
    return parts.reshape(-1, *shard.shape)


def sum_by_parts(shard, axes, sequence):
    size, lines = (lax.axis_size(axes), shard.reshape(-1, *shard.shape[1:][-1:]))
    parts = padded_to(lines, size).reshape(size, -1, *lines.shape[1:])
    own = own_block(parts, axes, sequence)
    whole = stacked_from(own, axes, sequence[::-1]).reshape(-1, *lines.shape[1:])
    return whole[: len(lines)].reshape(shard.shape)


def of_everyone(shard, axis):
    everything = sent_to_all(shard, axis)
    return jnp.sum(everything, axis=0)


def in_one(arrays, axis):
    ends = [0]
    for a in arrays:
        ends.append(ends[-1] + a.size)
    running = of_everyone(jnp.concatenate([a.ravel() for a in arrays]), axis)
    return tuple((running[b:e].reshape(a.shape) for a, b, e in zip(arrays, ends, ends[1:])))


def in_order(parts, dim):
    parts = jnp.moveaxis(parts, 0, dim)
    shape = parts.shape
    return parts.reshape(*shape[:dim], shape[dim] * shape[dim + 1], *shape[dim + 2 :])


def gather_packed(arrays, axis, dims):
    flat = jnp.concatenate([a.reshape(-1) for a in arrays])
    lines, at, done = (lax.all_gather(flat, axis), 0, [])
    for a, dim in zip(arrays, dims):
        parts = lines[:, at : at + a.size].reshape(-1, *a.shape)
        done.append(in_order(parts, dim))
        at += a.size
    return tuple(done)


def contract_rows(left, right):
    return lax.dot_general(
        left.astype(jnp.float32),
        right.astype(jnp.float32),
        (((0,), (0,)), ((), ())),
        preferred_element_type=jnp.float32,
        precision=lax.Precision.HIGHEST,
    )


def moments(first, second, projected):
    first_new = BETA_ONE * first + (1.0 - BETA_ONE) * projected
    second_new = BETA_TWO * second + (1.0 - BETA_TWO) * projected * projected
    normalized = first_new / (jnp.sqrt(second_new) + EPSILON)
    return (first_new, second_new, normalized)


def per_device(
    normed_input,
    value_cotangent,
    mixer_output,
    output_cotangent,
    value_factor,
    output_factor,
    value_master,
    value_moment,
    value_second,
    output_master,
    output_moment,
    output_second,
):
    highest = lax.Precision.HIGHEST
    row_index = lax.axis_index(FS)
    column_index = lax.axis_index("tp")
    value_rows = value_master.shape[0]
    output_rows = output_master.shape[0]
    factor_here = lax.dynamic_slice_in_dim(
        value_factor, row_index * value_rows, value_rows, 0
    ).astype(jnp.float32)
    feature_cols = normed_input.shape[1]
    factor_features = lax.dynamic_slice_in_dim(
        value_factor, column_index * feature_cols, feature_cols, 0
    )
    input_partial = jnp.dot(normed_input, factor_features, preferred_element_type=jnp.float32)
    input_reduced = taken_together(input_partial.astype(jnp.bfloat16), "tp").astype(jnp.float32)
    value_partial = contract_rows(input_reduced, value_cotangent)
    head_cols = mixer_output.shape[1]
    factor_heads = lax.dynamic_slice_in_dim(output_factor, column_index * head_cols, head_cols, 0)
    mixer_partial = jnp.dot(mixer_output, factor_heads, preferred_element_type=jnp.float32).astype(
        jnp.bfloat16
    )
    mixer_partial = lax.optimization_barrier(mixer_partial)
    mixer_reduced = (
        taken_together(mixer_partial.astype(jnp.float32).astype(jnp.bfloat16), "tp")
        .astype(jnp.float32)
        .astype(jnp.bfloat16)
    )
    output_partial = contract_rows(mixer_reduced, output_cotangent)
    value_projected, output_projected = (
        sum_by_parts(value_partial, FS, (0, 1)),
        sum_by_parts(output_partial, FS, (0, 1)),
    )
    value_moment_new, value_second_new, value_norm = moments(
        value_moment, value_second, value_projected
    )
    output_moment_new, output_second_new, output_norm = moments(
        output_moment, output_second, output_projected
    )
    value_total, output_total = in_one(
        (jnp.sum(value_norm * value_norm), jnp.sum(output_norm * output_norm)), "tp"
    )
    value_scale = lax.rsqrt(value_total / (R * WIDTH) + FLOOR)
    output_scale = lax.rsqrt(output_total / (R * D) + FLOOR)
    value_step = value_scale * jnp.dot(factor_here, value_norm, precision=highest)
    output_factor_rows = lax.dynamic_slice_in_dim(
        output_factor, row_index * output_rows, output_rows, 0
    ).astype(jnp.float32)
    output_step = output_scale * jnp.dot(output_factor_rows, output_norm, precision=highest)
    value_new = value_master - STEP_RATE * value_step
    output_new = output_master - STEP_RATE * output_step
    value_copy, output_copy = gather_packed(
        (value_new.astype(jnp.bfloat16), output_new.astype(jnp.bfloat16)), FS, (0, 0)
    )
    return (
        value_step,
        value_new,
        value_copy,
        value_moment_new,
        value_second_new,
        output_step,
        output_new,
        output_copy,
        output_moment_new,
        output_second_new,
    )


def solution(mesh):
    finer = Mesh(mesh.devices.reshape(16, 4, mesh.shape["tp"]), ("fs_0", "fs_1", "tp"))
    placed = (
        P(FS, "tp"),
        P(FS, "tp"),
        P(FS, "tp"),
        P(FS, "tp"),
        P(),
        P(),
        P(FS, "tp"),
        P(None, "tp"),
        P(None, "tp"),
        P(FS, "tp"),
        P(None, "tp"),
        P(None, "tp"),
    )
    return jax.shard_map(
        per_device,
        mesh=finer,
        in_specs=placed,
        out_specs=(
            P(FS, "tp"),
            P(FS, "tp"),
            P(None, "tp"),
            P(None, "tp"),
            P(None, "tp"),
            P(FS, "tp"),
            P(FS, "tp"),
            P(None, "tp"),
            P(None, "tp"),
            P(None, "tp"),
        ),
        check_vma=False,
    )
```

profile of v0, /device:TPU:1, one launch (start us, length us, event | category | flops | bytes accessed | tf_op | source)
XLA Modules:
  0.0 465.8 jit_solution(13149735531977660443)
XLA Ops:
  7.2 1.3 fusion.1
  8.7 1.1 broadcast_in_dim.10
  9.8 10.3 %all-to-all-start.1 = ((bf16[8,512,128]{2,1,0:T(8,128)(2,1)}), bf16[8,512,128]{2,1,0:T(8,128)(2,1)S(1)}, u32[]{:S(2)}, u32[]{:S(2)}) async-start(bf16[8,512,128]{2,1,0:T(8,128)(2,1)} %broadcast_in_dim.10), calls=%async_computation.1 | async-start | bytes 2097152 | tf_op jit(solution)/shard_map/all_to_all | solution.py:22
  20.5 14.5 %all-to-all-done.1 = bf16[8,512,128]{2,1,0:T(8,128)(2,1)S(1)} async-done(((bf16[8,512,128]{2,1,0:T(8,128)(2,1)}), bf16[8,512,128]{2,1,0:T(8,128)(2,1)S(1)}, u32[]{:S(2)}, u32[]{:S(2)}) %all-to-all-start.1) | async-done | bytes 1048608 | tf_op jit(solution)/shard_map/all_to_all | solution.py:22
  35.1 1.1 broadcast_in_dim.9
  36.2 4.4 all-to-all-start
  41.0 14.6 %all-to-all-done = bf16[8,512,128]{2,1,0:T(8,128)(2,1)S(1)} async-done(((bf16[8,512,128]{2,1,0:T(8,128)(2,1)}), bf16[8,512,128]{2,1,0:T(8,128)(2,1)S(1)}, u32[]{:S(2)}, u32[]{:S(2)}) %all-to-all-start) | async-done | bytes 1048608 | tf_op jit(solution)/shard_map/all_to_all | solution.py:22
  56.1 0.9 fusion.2
  57.0 1.0 fusion.5
  58.0 1.3 dynamic-slice.2
  59.3 1.3 dynamic-slice
  61.2 123.2 %all-reduce.8.cloned.1.call-done = (f32[64,2,512]{2,0,1:T(8,128)}, f32[64,2,256]{2,0,1:T(8,128)}) async-done(((f32[64,2,512]{2,0,1:T(8,128)}, f32[64,2,256]{2,0,1:T(8,128)}), (f32[64,2,512]{2,0,1:T(8,128)}, f32[64,2,256]{2,0,1:T(8,128)})) %all-reduce.8.cloned.1.call-update) | async-done | bytes 393232
  184.4 0.8 constant_dynamic-slice_fusion.1
  185.1 0.7 constant_dynamic-slice_fusion.3
  185.9 13.3 %all-reduce.5 = (f32[4,2,512]{2,1,0:T(2,128)S(1)}, f32[4,2,256]{2,1,0:T(2,128)S(1)}) all-reduce(f32[4,2,512]{2,1,0:T(2,128)S(1)} %copy.51, f32[4,2,256]{2,1,0:T(2,128)S(1)} %copy.47), channel_id=8, replica_groups=mesh['fs_0'=16,'fs_1'=4,'tp'=8] {'fs_1'}, use_global_device_ids=true, to_apply=%region_6.0.clone | all-reduce | flops 6144 | bytes 49152
  199.1 0.7 constant_dynamic-slice_fusion
  199.8 0.7 constant_dynamic-slice_fusion.2
  200.5 8.1 %all_gather.24 = f32[4,2,256]{2,1,0:T(2,128)S(1)} all-gather(f32[1,2,256]{2,1,0:T(2,128)S(1)} %constant_dynamic-slice_fusion.2), channel_id=1, replica_groups=mesh['fs_0'=16,'fs_1'=4,'tp'=8] {'fs_1'}, dimensions={0}, use_global_device_ids=true | all-gather | bytes 10240 | tf_op jit(solution)/shard_map/all_gather | solution.py:48
  208.6 9.1 %all_gather.27 = f32[4,2,512]{2,1,0:T(2,128)S(1)} all-gather(f32[1,2,512]{2,1,0:T(2,128)S(1)} %constant_dynamic-slice_fusion), channel_id=1, replica_groups=mesh['fs_0'=16,'fs_1'=4,'tp'=8] {'fs_1'}, dimensions={0}, use_global_device_ids=true | all-gather | bytes 20480 | tf_op jit(solution)/shard_map/all_gather | solution.py:48
  217.7 21.7 %all-gather = f32[64,2,256]{2,1,0:T(2,128)S(1)} all-gather(f32[4,2,256]{2,1,0:T(2,128)S(1)} %all_gather.24), channel_id=2, replica_groups=mesh['fs_0'=16,'fs_1'=4,'tp'=8] {'fs_0'}, dimensions={0}, use_global_device_ids=true | all-gather | bytes 139264 | tf_op jit(solution)/shard_map/all_gather | solution.py:48
  239.5 20.5 %all-gather.1 = f32[64,2,512]{2,1,0:T(2,128)S(1)} all-gather(f32[4,2,512]{2,1,0:T(2,128)S(1)} %all_gather.27), channel_id=3, replica_groups=mesh['fs_0'=16,'fs_1'=4,'tp'=8] {'fs_0'}, dimensions={0}, use_global_device_ids=true | all-gather | bytes 278528 | tf_op jit(solution)/shard_map/all_gather | solution.py:48
  260.2 0.7 multiply_reduce_fusion.1
  260.9 0.8 multiply_reduce_fusion
  261.7 1.4 pad_maximum_fusion.1
  263.6 37.4 %all-to-all-start.2 = ((f32[8,1,2]{2,1,0:T(1,128)}), f32[8,1,2]{2,1,0:T(1,128)S(1)}, u32[]{:S(2)}, u32[]{:S(2)}) async-start(f32[8,1,2]{2,1,0:T(1,128)} %broadcast_in_dim.11), calls=%async_computation.2 | async-start | bytes 8192 | tf_op jit(solution)/shard_map/all_to_all | solution.py:22
  301.0 4.5 all-to-all-done.2
  308.5 1.0 convolution_multiply_fusion
  310.9 130.3 %all-gather.5.cloned.1.call-done = bf16[2097152]{0:T(1024)(128)(2,1)} async-done(((bf16[32768]{0:T(1024)(128)(2,1)}), bf16[2097152]{0:T(1024)(128)(2,1)}) %all-gather.5.cloned.1.call-update) | async-done | bytes 4194320 | tf_op jit(solution)/shard_map/all_gather | solution.py:84
  441.2 7.4 %reshape.56 = bf16[64,32768]{1,0:T(8,128)(2,1)} reshape(bf16[2097152]{0:T(1024)(128)(2,1)} %all-gather.5.cloned.1.call-done) | data formatting | bytes 8388608 | tf_op jit(solution)/shard_map/all_gather | solution.py:84
  448.6 3.9 fusion.20
  452.4 4.2 reshape_reshape.15
  456.6 2.3 reshape_reshape.14
  (58 shorter events, 5.1 us)
Async XLA Ops:
  7.2 12.9 %copy-start = (bf16[4096,128]{1,0:T(8,128)(2,1)S(1)}, bf16[4096,128]{1,0:T(8,128)(2,1)}, u32[]{:S(2)}) copy-start(bf16[4096,128]{1,0:T(8,128)(2,1)} %param.16) | copy-start | bytes 3145732
  7.2 12.9 %copy-start.2 = (bf16[512,512]{1,0:T(8,128)(2,1)S(1)}, bf16[512,512]{1,0:T(8,128)(2,1)}, u32[]{:S(2)}) copy-start(bf16[512,512]{1,0:T(8,128)(2,1)} %param.12) | copy-start | bytes 1572868
  9.8 25.3 %all-to-all-start.1 = ((bf16[8,512,128]{2,1,0:T(8,128)(2,1)}), bf16[8,512,128]{2,1,0:T(8,128)(2,1)S(1)}, u32[]{:S(2)}, u32[]{:S(2)}) async-start(bf16[8,512,128]{2,1,0:T(8,128)(2,1)} %broadcast_in_dim.10), calls=%async_computation.1 | async-start | bytes 2097152 | tf_op jit(solution)/shard_map/all_to_all | solution.py:22
  36.2 19.4 %all-to-all-start = ((bf16[8,512,128]{2,1,0:T(8,128)(2,1)}), bf16[8,512,128]{2,1,0:T(8,128)(2,1)S(1)}, u32[]{:S(2)}, u32[]{:S(2)}) async-start(bf16[8,512,128]{2,1,0:T(8,128)(2,1)} %broadcast_in_dim.9), calls=%async_computation | async-start | bytes 2097152 | tf_op jit(solution)/shard_map/all_to_all | solution.py:22
  40.6 143.8 %all-reduce.8.cloned.1.call-start = ((), (), s32[]{:S(2)}) async-start(), calls=%async_computation.4 | async-start | bytes 786432
  40.8 15.3 %copy-start.1 = (bf16[512,512]{1,0:T(8,128)(2,1)S(1)}, bf16[512,512]{1,0:T(8,128)(2,1)}, u32[]{:S(2)}) copy-start(bf16[512,512]{1,0:T(8,128)(2,1)} %param.15) | copy-start | bytes 1572868
  40.8 16.3 %copy-start.7 = (bf16[512,256]{1,0:T(8,128)(2,1)S(1)}, bf16[512,256]{1,0:T(8,128)(2,1)}, u32[]{:S(2)}) copy-start(bf16[512,256]{1,0:T(8,128)(2,1)} %param.13) | copy-start | bytes 786436
  55.9 204.3 %copy-start.8 = (f32[128,256]{1,0:T(8,128)S(1)}, f32[128,256]{1,0:T(8,128)}, u32[]{:S(2)}) copy-start(f32[128,256]{1,0:T(8,128)} %param.20) | copy-start | bytes 393220
  55.9 204.3 %copy-start.9 = (f32[128,256]{1,0:T(8,128)S(1)}, f32[128,256]{1,0:T(8,128)}, u32[]{:S(2)}) copy-start(f32[128,256]{1,0:T(8,128)} %param.19) | copy-start | bytes 393220
  56.1 204.8 %copy-start.3 = (f32[128,512]{1,0:T(8,128)S(1)}, f32[128,512]{1,0:T(8,128)}, u32[]{:S(2)}) copy-start(f32[128,512]{1,0:T(8,128)} %param.23) | copy-start | bytes 786436
  56.1 204.8 %copy-start.4 = (f32[128,512]{1,0:T(8,128)S(1)}, f32[128,512]{1,0:T(8,128)}, u32[]{:S(2)}) copy-start(f32[128,512]{1,0:T(8,128)} %param.22) | copy-start | bytes 786436
  58.0 249.8 %copy-start.12 = (f32[64,256]{1,0:T(8,128)S(1)}, f32[64,256]{1,0:T(8,128)}, u32[]{:S(2)}) copy-start(f32[64,256]{1,0:T(8,128)} %param.18) | copy-start | bytes 196612
  260.0 49.6 %copy-start.13 = (f32[32,512]{1,0:T(8,128)S(1)}, f32[32,512]{1,0:T(8,128)}, u32[]{:S(2)}) copy-start(f32[32,512]{1,0:T(8,128)} %param.21) | copy-start | bytes 196612
  260.9 180.3 %copy-start.11 = (f32[128,256]{1,0:T(8,128)}, f32[128,256]{1,0:T(8,128)S(1)}, u32[]{:S(2)}) copy-start(f32[128,256]{1,0:T(8,128)S(1)} %get-tuple-element.20) | copy-start | bytes 393220
  260.9 187.7 %copy-start.10 = (f32[128,256]{1,0:T(8,128)}, f32[128,256]{1,0:T(8,128)S(1)}, u32[]{:S(2)}) copy-start(f32[128,256]{1,0:T(8,128)S(1)} %get-tuple-element.19) | copy-start | bytes 393220
  261.7 179.5 %copy-start.6 = (f32[128,512]{1,0:T(8,128)}, f32[128,512]{1,0:T(8,128)S(1)}, u32[]{:S(2)}) copy-start(f32[128,512]{1,0:T(8,128)S(1)} %get-tuple-element.23) | copy-start | bytes 786436
  261.7 186.9 %copy-start.5 = (f32[128,512]{1,0:T(8,128)}, f32[128,512]{1,0:T(8,128)S(1)}, u32[]{:S(2)}) copy-start(f32[128,512]{1,0:T(8,128)S(1)} %get-tuple-element.22) | copy-start | bytes 786436
  263.6 41.9 %all-to-all-start.2 = ((f32[8,1,2]{2,1,0:T(1,128)}), f32[8,1,2]{2,1,0:T(1,128)S(1)}, u32[]{:S(2)}, u32[]{:S(2)}) async-start(f32[8,1,2]{2,1,0:T(1,128)} %broadcast_in_dim.11), calls=%async_computation.2 | async-start | bytes 8192 | tf_op jit(solution)/shard_map/all_to_all | solution.py:22
  301.0 140.1 %all-gather.5.cloned.1.call-start = ((), (), s32[]{:S(2)}) async-start(), calls=%async_computation.3 | async-start | bytes 4259840 | tf_op jit(solution)/shard_map/all_gather | solution.py:84
  307.8 133.4 %copy-start.14 = (f32[64,256]{1,0:T(8,128)}, f32[64,256]{1,0:T(8,128)S(1)}, u32[]{:S(2)}) copy-start(f32[64,256]{1,0:T(8,128)S(1)} %convolution_multiply_fusion.1) | copy-start | bytes 196612
  309.5 131.6 %copy-start.15 = (f32[32,512]{1,0:T(8,128)}, f32[32,512]{1,0:T(8,128)S(1)}, u32[]{:S(2)}) copy-start(f32[32,512]{1,0:T(8,128)S(1)} %convolution_multiply_fusion) | copy-start | bytes 196612
Sparse Core Ops, SparseCore 0:
  58.1 126.1 all-reduce.7
  311.0 130.1 all-gather.4
where the time goes:
time: 475 us; the launch traced here: 466 us
  waiting for transfers between devices  287 us (60%)
  blocking collectives  72.7 us (15%)
  starting transfers between devices  52.1 us (11%)
  local copies, waits for them, and re-layouts  27.6 us (6%)
  between operations  16.3 us (3%)
  other arithmetic  5.08 us (1%)
  matrix products  4.78 us (1%)
    all_gather x1, waiting for transfers between devices, gather_packed(): lines, at, done = (lax.all_gather(flat, axis), 0, [])  130 us
    unnamed x3, waiting for transfers between devices  123 us
    all_gather x4, blocking collectives, stacked_from(): parts = lax.all_gather(parts, axes[k])  59.4 us
    all_to_all x3, starting transfers between devices, sent_to_all(): return lax.all_to_all(copies, axis, split_axis=0, concat_axis=0, tiled=True)  52.1 us
    all_to_all x3, waiting for transfers between devices, sent_to_all(): return lax.all_to_all(copies, axis, split_axis=0, concat_axis=0, tiled=True)  33.7 us
    unnamed x1, blocking collectives  13.3 us
  transfers between devices with their start and end apart: 5, of which 5 were waited for; matrix products, arithmetic and copies ran while one was open for 1% of the time, Pallas kernels for 0%

commit v1 on v0

v1 whole, which is shorter than its diff:
```python
import jax
import jax.numpy as jnp
from jax import lax
from jax.experimental import pallas as pl
from jax.experimental.pallas import tpu as pltpu
from jax.sharding import Mesh
from jax.sharding import PartitionSpec as P

D = 4096
WIDTH = 2048
R = 128
TOK = 512
NZ, NY, NT = 16, 4, 8
FEAT = D // NT
HEAD = WIDTH // NT
VC = WIDTH // NT
OC = D // NT
PC = VC + OC
VROWS = D // (NZ * NY)
OROWS = WIDTH // (NZ * NY)
BLK = VROWS + 2 * OROWS
ASPLIT = 48
BHALF = 96

BETA_ONE = 0.8
BETA_TWO = 0.9
EPSILON = 1e-08
STEP_RATE = 0.005
FLOOR = 0.25

BF = jnp.bfloat16
F32 = jnp.float32
MESH = pl.DeviceIdType.MESH


def moments(first, second, projected):
    first_new = BETA_ONE * first + (1.0 - BETA_ONE) * projected
    second_new = BETA_TWO * second + (1.0 - BETA_TWO) * projected * projected
    normalized = first_new / (jnp.sqrt(second_new) + EPSILON)
    return first_new, second_new, normalized


def exchange_kernel(
    n_in, vc_in, mo_in, oc_in, fv_in, fo_in, vw_in, vm_in, vs_in, ow_in, om_in, os_in,
    g_out, p_out, s_out,
    nb, vcb, mob, ocb, fvb, fob, vwb, vmb, vsb, owb, omb, osb,
    xs, xr, xg, pf, pb, yr, zs, zb, zr, zg, nat, yg, st, sr, g,
    lsem, osem,
    xs_s, xs_r, xg_s, xg_r, sc_s, sc_r, yr_s, yr_r, yg_s, yg_r,
    zr_s, zr_r, zg_s, zg_r, ay_s, ay_r, az_s, az_r, bz_s, bz_r, by_s, by_r,
):
    z, y, t = lax.axis_index("z"), lax.axis_index("y"), lax.axis_index("tp")

    def around(k, i, n):
        return lax.rem(k + (i + n), n)

    barrier = pltpu.get_barrier_semaphore()
    for i in range(1, NT):
        pl.semaphore_signal(barrier, inc=1, device_id={"tp": around(t, i, NT)}, device_id_type=MESH)
    for i in range(1, NY):
        pl.semaphore_signal(barrier, inc=1, device_id={"y": around(y, i, NY)}, device_id_type=MESH)
    for i in range(1, NZ):
        pl.semaphore_signal(barrier, inc=1, device_id={"z": around(z, i, NZ)}, device_id_type=MESH)

    loads = []
    for k, (src, dst) in enumerate((
        (vw_in, vwb), (ow_in, owb),
        (fv_in.at[pl.ds(pl.multiple_of(t * FEAT, FEAT), FEAT)], fvb), (n_in, nb),
        (fo_in.at[pl.ds(pl.multiple_of(t * HEAD, HEAD), HEAD)], fob), (mo_in, mob),
        (vc_in, vcb), (oc_in, ocb),
        (vm_in, vmb), (vs_in, vsb), (om_in, omb), (os_in, osb),
    )):
        c = pltpu.make_async_copy(src, dst, lsem.at[k])
        c.start()
        loads.append(c)

    sent = []

    def remote(src, dst, ssem, rsem, **where):
        c = pltpu.make_async_remote_copy(
            src_ref=src, dst_ref=dst, send_sem=ssem, recv_sem=rsem,
            device_id=where, device_id_type=MESH,
        )
        return c

    def send(src, dst, ssem, rsem, **where):
        c = remote(src, dst, ssem, rsem, **where)
        c.start()
        sent.append(c)

    def arrived(dst, rsem):
        remote(dst, dst, rsem, rsem, tp=t).wait_recv()

    for c in loads[:2]:
        c.wait()
    g[z, y, 0:VROWS, :] = vwb[...].astype(BF)
    g[z, y, VROWS:VROWS + OROWS, :] = owb[:, 0:VC].astype(BF)
    g[z, y, VROWS + OROWS:BLK, :] = owb[:, VC:OC].astype(BF)
    for c in loads[2:4]:
        c.wait()
    nt = (((1,), (1,)), ((), ()))
    part = lax.dot_general(fvb[...].T, nb[...], nt, preferred_element_type=F32)
    xs[:, 0:16, :] = part.astype(BF).reshape(NT, 16, TOK)
    for c in loads[4:6]:
        c.wait()
    part = lax.dot_general(fob[...].T, mob[...], nt, preferred_element_type=F32)
    xs[:, 16:32, :] = part.astype(BF).reshape(NT, 16, TOK)

    def a_rows(k, ys=None):
        return g.at[k, :, pl.ds(0, ASPLIT), :] if ys is None else g.at[k, pl.ds(ys, NY // 2), pl.ds(0, ASPLIT), :]

    def b_rows(k, j=None, part=None):
        lo, hi = {None: (ASPLIT, BLK), 0: (ASPLIT, BHALF), 1: (BHALF, BLK)}[part]
        return g.at[k, y if j is None else j, pl.ds(lo, hi - lo), :]

    LAST = NZ // 2
    up, down = around(z, 1, NZ), around(z, -1, NZ)
    yup, ydown = around(y, 1, NY), around(y, -1, NY)

    def a_begin():
        own = g.at[z, y, pl.ds(0, ASPLIT), :]
        for i in range(1, NY):
            send(own, own, ay_s.at[i], ay_r.at[i], y=around(y, i, NY))

    def a_ring(s):
        if s == 0:
            for i in range(1, NY):
                arrived(g.at[z, around(y, -i, NY), pl.ds(0, ASPLIT), :], ay_r.at[i])
        below, above = around(z, -s, NZ), around(z, s, NZ)
        if 0 < s < LAST:
            arrived(a_rows(below), az_r.at[0, s])
            arrived(a_rows(above), az_r.at[1, s])
        if s == LAST:
            arrived(a_rows(below, 0), az_r.at[0, s])
            arrived(a_rows(above, NY // 2), az_r.at[1, s])
            return
        half = s + 1 == LAST
        for d, (k, to) in enumerate(((below, up), (above, down))):
            block = a_rows(k, d * (NY // 2)) if half else a_rows(k)
            send(block, block, az_s.at[d, s + 1], az_r.at[d, s + 1], z=to)

    def b_across(k, b):
        block = b_rows(k)
        send(block, block, by_s.at[0, b], by_r.at[0, b], y=yup)
        send(block, block, by_s.at[1, b], by_r.at[1, b], y=ydown)

    def b_ids(s):
        if s == 0:
            return ((0, 0),)
        if s == LAST:
            return ((LAST, NZ - 1),)
        return ((-s, 2 * s - 1), (s, 2 * s))

    def b_ring(s):
        below, above = around(z, -s, NZ), around(z, s, NZ)
        if 0 < s < LAST:
            arrived(b_rows(below), bz_r.at[0, s])
            arrived(b_rows(above), bz_r.at[1, s])
        if s == LAST:
            arrived(b_rows(below, part=0), bz_r.at[0, s])
            arrived(b_rows(above, part=1), bz_r.at[1, s])
        else:
            half = s + 1 == LAST
            for d, (k, to) in enumerate(((below, up), (above, down))):
                block = b_rows(k, part=d) if half else b_rows(k)
                send(block, block, bz_s.at[d, s + 1], bz_r.at[d, s + 1], z=to)
        for off, b in b_ids(s):
            b_across(around(z, off, NZ), b)

    def b_forward(s):
        for off, b in b_ids(s):
            k = around(z, off, NZ)
            arrived(b_rows(k, ydown), by_r.at[0, b])
            block = b_rows(k, ydown, 0)
            send(block, block, by_s.at[2, b], by_r.at[2, b], y=yup)
            arrived(b_rows(k, yup), by_r.at[1, b])
            block = b_rows(k, yup, 1)
            send(block, block, by_s.at[3, b], by_r.at[3, b], y=ydown)

    writes = []

    def b_end(s):
        across = around(y, 2, NY)
        for off, b in b_ids(s):
            k = around(z, off, NZ)
            arrived(b_rows(k, across, 0), by_r.at[2, b])
            arrived(b_rows(k, across, 1), by_r.at[3, b])
            c = pltpu.make_async_copy(g.at[k], g_out.at[k], osem.at[b])
            c.start()
            writes.append(c)

    pl.semaphore_wait(barrier, NT + NY + NZ - 3)

    def c_scatter():
        for i in range(1, NT):
            to = around(t, i, NT)
            send(xs.at[to], xr.at[i], xs_s.at[i], xs_r.at[i], tp=to)

    def c_gather():
        for i in range(1, NT):
            arrived(xr.at[i], xs_r.at[i])
        total = xs[t].astype(F32)
        for i in range(1, NT):
            total = total + xr[i].astype(F32)
        xg[t] = total.astype(BF)
        for i in range(1, NT):
            send(xg.at[t], xg.at[t], xg_s.at[i], xg_r.at[i], tp=around(t, i, NT))

    def c_project():
        for c in loads[6:8]:
            c.wait()
        for i in range(1, NT):
            arrived(xg.at[around(t, -i, NT)], xg_r.at[i])
        left = xg[:, 0:16, :].reshape(R, TOK)
        right = xg[:, 16:32, :].reshape(R, TOK)
        pv = jnp.dot(left, vcb[...], preferred_element_type=F32).reshape(NY, R // NY, VC)
        po = jnp.dot(right, ocb[...], preferred_element_type=F32).reshape(NY, R // NY, OC)
        pf[:, :, 0:VC] = pv
        pf[:, :, VC:PC] = po
        pb[:, :, 0:VC] = pv.astype(BF)
        pb[:, :, VC:PC] = po.astype(BF)
        for i in range(1, NY):
            to = around(y, i, NY)
            send(pb.at[to], yr.at[i], yr_s.at[i], yr_r.at[i], y=to)

    def c_zscatter():
        for i in range(1, NY):
            arrived(yr.at[i], yr_r.at[i])
        total = pf[y]
        for i in range(1, NY):
            total = total + yr[i].astype(F32)
        for k in range(NZ):
            q, r = divmod(k, 4)
            zs[k, 0:8, :] = total[8 * q:8 * q + 8, VC + 128 * r:VC + 128 * r + 128]
            q, r = divmod(k, 2)
            zs[k, 8:12, :] = total[4 * q:4 * q + 4, 128 * r:128 * r + 128]
            zs[k, 12:16, :] = jnp.zeros((4, 128), F32)
        zb[...] = zs[...].astype(BF)
        for i in range(1, NZ):
            to = around(z, i, NZ)
            send(zb.at[to], zr.at[i], zr_s.at[i], zr_r.at[i], z=to)

    def c_zgather():
        for i in range(1, NZ):
            arrived(zr.at[i], zr_r.at[i])
        total = zs[z]
        for i in range(1, NZ):
            total = total + zr[i].astype(F32)
        zg[z] = total.astype(BF)
        for i in range(1, NZ):
            send(zg.at[z], zg.at[z], zg_s.at[i], zg_r.at[i], z=around(z, i, NZ))

    def c_ygather():
        for i in range(1, NZ):
            arrived(zg.at[around(z, -i, NZ)], zg_r.at[i])
        for k in range(NZ):
            chunk = zg[k].astype(F32)
            q, r = divmod(k, 4)
            nat[8 * q:8 * q + 8, VC + 128 * r:VC + 128 * r + 128] = chunk[0:8]
            q, r = divmod(k, 2)
            nat[4 * q:4 * q + 4, 128 * r:128 * r + 128] = chunk[8:12]
        yg[y] = nat[...].astype(BF)
        for i in range(1, NY):
            send(yg.at[y], yg.at[y], yg_s.at[i], yg_r.at[i], y=around(y, i, NY))

    def c_squares():
        for c in loads[8:12]:
            c.wait()
        for i in range(1, NY):
            arrived(yg.at[around(y, -i, NY)], yg_r.at[i])
        c = pltpu.make_async_copy(yg, p_out, osem.at[NZ])
        c.start()
        writes.append(c)
        whole = yg[...].reshape(R, PC).astype(F32)
        _, _, vn = moments(vmb[...], vsb[...], whole[:, 0:VC])
        _, _, on = moments(omb[...], osb[...], whole[:, VC:PC])
        row = lax.broadcasted_iota(jnp.int32, (8, 128), 0)
        st[...] = jnp.where(row < 4, jnp.sum(vn * vn), jnp.sum(on * on))
        for i in range(1, NT):
            send(st, sr.at[i], sc_s.at[i], sc_r.at[i], tp=around(t, i, NT))

    def c_scales():
        for i in range(1, NT):
            arrived(sr.at[i], sc_r.at[i])
        total = st[...]
        for i in range(1, NT):
            total = total + sr[i]
        row = lax.broadcasted_iota(jnp.int32, (8, 128), 0)
        mean = total * jnp.where(row < 4, 1.0 / (R * WIDTH), 1.0 / (R * D)).astype(F32)
        sr[0] = lax.rsqrt(mean + FLOOR)
        c = pltpu.make_async_copy(sr.at[0], s_out, osem.at[NZ + 1])
        c.start()
        writes.append(c)

    c_scatter()
    a_begin()
    b_ring(0)
    a_ring(0)
    b_ring(1)
    b_forward(0)
    c_gather()
    a_ring(1)
    b_ring(2)
    b_forward(1)
    b_end(0)
    c_project()
    a_ring(2)
    b_ring(3)
    b_forward(2)
    b_end(1)
    c_zscatter()
    a_ring(3)
    b_ring(4)
    b_forward(3)
    b_end(2)
    a_ring(4)
    b_ring(5)
    b_forward(4)
    b_end(3)
    c_zgather()
    a_ring(5)
    b_ring(6)
    b_forward(5)
    b_end(4)
    a_ring(6)
    b_ring(7)
    b_forward(6)
    b_end(5)
    c_ygather()
    a_ring(7)
    b_ring(8)
    b_forward(7)
    b_end(6)
    c_squares()
    b_forward(8)
    b_end(7)
    a_ring(8)
    b_end(8)
    c_scales()
    for c in writes:
        c.wait()
    for c in sent:
        c.wait_send()


def update_kernel(
    g_in, p_in, s_in, fv_in, fo_in, vw_in, vm_in, vs_in, ow_in, om_in, os_in,
    vstep_out, vnew_out, vcopy_out, vm_out, vs_out, ostep_out, onew_out, ocopy_out, om_out, os_out,
    gb, pbuf, sbuf, fvb, fob, vwb, vmb, vsb, owb, omb, osb,
    vstep, vnew, vcopy, ostep, onew, ocopy, fvh, foh,
    lsem, gsem, fvsem, fosem, wsem, vcsem, ocsem,
):
    z, y = lax.axis_index("z"), lax.axis_index("y")
    row = z * NY + y

    loads = []
    for k, (src, dst) in enumerate((
        (p_in, pbuf), (s_in, sbuf), (vm_in, vmb), (vs_in, vsb), (om_in, omb), (os_in, osb),
        (vw_in, vwb), (ow_in, owb),
        (fv_in.at[pl.ds(pl.multiple_of(row * VROWS, VROWS), VROWS)], fvh),
        (fo_in.at[pl.ds(pl.multiple_of(row * OROWS, OROWS), OROWS)], foh),
    )):
        c = pltpu.make_async_copy(src, dst, lsem.at[k])
        c.start()
        loads.append(c)
    fv_load = pltpu.make_async_copy(fv_in, fvb, fvsem)
    fo_load = pltpu.make_async_copy(fo_in, fob, fosem)
    fv_load.start()
    fo_load.start()
    g_loads = [pltpu.make_async_copy(g_in.at[k], gb.at[k], gsem.at[k]) for k in range(NZ)]
    for c in g_loads:
        c.start()

    for c in loads:
        c.wait()
    p = pbuf[...].reshape(R, PC).astype(F32)
    vm, vs, vn = moments(vmb[...], vsb[...], p[:, 0:VC])
    om, os, on = moments(omb[...], osb[...], p[:, VC:PC])
    vmb[...] = vm
    vsb[...] = vs
    omb[...] = om
    osb[...] = os
    writes = []

    def write(src, dst, sem):
        c = pltpu.make_async_copy(src, dst, sem)
        c.start()
        writes.append(c)

    for k, (src, dst) in enumerate(((vmb, vm_out), (vsb, vs_out), (omb, om_out), (osb, os_out))):
        write(src, dst, wsem.at[k])
    v_scale = sbuf[0:1, 0:1]
    o_scale = sbuf[4:5, 0:1]
    highest = lax.Precision.HIGHEST
    vstep[...] = v_scale * jnp.dot(fvh[...].astype(F32), vn, precision=highest, preferred_element_type=F32)
    ostep[...] = o_scale * jnp.dot(foh[...].astype(F32), on, precision=highest, preferred_element_type=F32)
    vnew[...] = vwb[...] - STEP_RATE * vstep[...]
    onew[...] = owb[...] - STEP_RATE * ostep[...]
    for k, (src, dst) in enumerate(((vstep, vstep_out), (vnew, vnew_out), (ostep, ostep_out), (onew, onew_out))):
        write(src, dst, wsem.at[4 + k])

    def two(normalized, scale):
        scaled = normalized * (scale * STEP_RATE)
        high = scaled.astype(BF)
        low = (scaled - high.astype(F32)).astype(BF)
        return jnp.concatenate([high, low], axis=0)

    v_two = two(vn, v_scale)
    o_two = two(on, o_scale)
    fv_load.wait()
    fo_load.wait()
    vt, ot = NY * VROWS, NY * OROWS
    for k in range(NZ):
        g_loads[k].wait()
        f = fvb[k * vt:(k + 1) * vt, :]
        delta = jnp.dot(jnp.concatenate([f, f], axis=1), v_two, preferred_element_type=F32)
        held = gb[k, :, 0:VROWS, :].reshape(vt, VC).astype(F32)
        vcopy[k * vt:(k + 1) * vt, :] = (held - delta).astype(BF)
        write(vcopy.at[pl.ds(k * vt, vt)], vcopy_out.at[pl.ds(k * vt, vt)], vcsem.at[k])
        f = fob[k * ot:(k + 1) * ot, :]
        delta = jnp.dot(jnp.concatenate([f, f], axis=1), o_two, preferred_element_type=F32)
        for h in range(2):
            lo = VROWS + h * OROWS
            held = gb[k, :, lo:lo + OROWS, :].reshape(ot, VC).astype(F32)
            ocopy[k * ot:(k + 1) * ot, h * VC:(h + 1) * VC] = (held - delta[:, h * VC:(h + 1) * VC]).astype(BF)
        write(ocopy.at[pl.ds(k * ot, ot)], ocopy_out.at[pl.ds(k * ot, ot)], ocsem.at[k])
    for c in writes:
        c.wait()


def per_device(
    normed_input, value_cotangent, mixer_output, output_cotangent, value_factor, output_factor,
    value_master, value_moment, value_second, output_master, output_moment, output_second,
):
    anywhere = pl.BlockSpec(memory_space=pl.ANY)
    dma = pltpu.SemaphoreType.DMA

    def vmem(shape, dtype):
        return pltpu.VMEM(shape, dtype)

    gathered, projected, scales = pl.pallas_call(
        exchange_kernel,
        name="exchange",
        out_shape=(
            jax.ShapeDtypeStruct((NZ, NY, BLK, VC), BF),
            jax.ShapeDtypeStruct((NY, R // NY, PC), BF),
            jax.ShapeDtypeStruct((8, 128), F32),
        ),
        in_specs=[anywhere] * 12,
        out_specs=(anywhere,) * 3,
        scratch_shapes=[
            vmem((TOK, FEAT), BF), vmem((TOK, VC), BF), vmem((TOK, HEAD), BF), vmem((TOK, OC), BF),
            vmem((FEAT, R), BF), vmem((HEAD, R), BF),
            vmem((VROWS, VC), F32), vmem((R, VC), F32), vmem((R, VC), F32),
            vmem((OROWS, OC), F32), vmem((R, OC), F32), vmem((R, OC), F32),
            vmem((NT, 32, TOK), BF), vmem((NT, 32, TOK), BF), vmem((NT, 32, TOK), BF),
            vmem((NY, R // NY, PC), F32), vmem((NY, R // NY, PC), BF), vmem((NY, R // NY, PC), BF),
            vmem((NZ, 16, 128), F32), vmem((NZ, 16, 128), BF), vmem((NZ, 16, 128), BF), vmem((NZ, 16, 128), BF),
            vmem((R // NY, PC), F32), vmem((NY, R // NY, PC), BF),
            vmem((8, 128), F32), vmem((NT, 8, 128), F32),
            vmem((NZ, NY, BLK, VC), BF),
            dma((12,)), dma((NZ + 2,)),
            dma((NT,)), dma((NT,)), dma((NT,)), dma((NT,)), dma((NT,)), dma((NT,)),
            dma((NY,)), dma((NY,)), dma((NY,)), dma((NY,)),
            dma((NZ,)), dma((NZ,)), dma((NZ,)), dma((NZ,)),
            dma((NY,)), dma((NY,)),
            dma((2, NZ // 2 + 1)), dma((2, NZ // 2 + 1)), dma((2, NZ // 2 + 1)), dma((2, NZ // 2 + 1)),
            dma((4, NZ)), dma((4, NZ)),
        ],
        compiler_params=pltpu.CompilerParams(collective_id=0, has_side_effects=True),
    )(
        normed_input, value_cotangent, mixer_output, output_cotangent, value_factor, output_factor,
        value_master, value_moment, value_second, output_master, output_moment, output_second,
    )

    def like(a, dtype=F32):
        return jax.ShapeDtypeStruct(a, dtype)

    return pl.pallas_call(
        update_kernel,
        name="update",
        out_shape=(
            like((VROWS, VC)), like((VROWS, VC)), like((D, VC), BF), like((R, VC)), like((R, VC)),
            like((OROWS, OC)), like((OROWS, OC)), like((WIDTH, OC), BF), like((R, OC)), like((R, OC)),
        ),
        in_specs=[anywhere] * 11,
        out_specs=(anywhere,) * 10,
        scratch_shapes=[
            vmem((NZ, NY, BLK, VC), BF), vmem((NY, R // NY, PC), BF), vmem((8, 128), F32),
            vmem((D, R), BF), vmem((WIDTH, R), BF),
            vmem((VROWS, VC), F32), vmem((R, VC), F32), vmem((R, VC), F32),
            vmem((OROWS, OC), F32), vmem((R, OC), F32), vmem((R, OC), F32),
            vmem((VROWS, VC), F32), vmem((VROWS, VC), F32), vmem((D, VC), BF),
            vmem((OROWS, OC), F32), vmem((OROWS, OC), F32), vmem((WIDTH, OC), BF),
            vmem((VROWS, R), BF), vmem((OROWS, R), BF),
            dma((10,)), dma((NZ,)), dma, dma, dma((8,)), dma((NZ,)), dma((NZ,)),
        ],
    )(
        gathered, projected, scales, value_factor, output_factor,
        value_master, value_moment, value_second, output_master, output_moment, output_second,
    )


def solution(mesh):
    finer = Mesh(mesh.devices.reshape(NZ, NY, NT), ("z", "y", "tp"))
    fs = ("z", "y")
    rows, cols = P(fs, "tp"), P(None, "tp")
    return jax.shard_map(
        per_device,
        mesh=finer,
        in_specs=(rows, rows, rows, rows, P(), P(), rows, cols, cols, rows, cols, cols),
        out_specs=(rows, rows, cols, cols, cols, rows, rows, cols, cols, cols),
        check_vma=False,
    )
```

time: 475 us -> 76.6 us (0.16); the launches traced: 466 us -> 76.5 us
  waiting for transfers between devices: 287 us -> 0 us
  Pallas kernels: 0 us -> 75.8 us
  blocking collectives: 72.7 us -> 0 us
  starting transfers between devices: 52.1 us -> 0 us
  local copies, waits for them, and re-layouts: 27.6 us -> 0 us
  between operations: 16.3 us -> 0.65 us
  other arithmetic: 5.08 us -> 0 us
  matrix products: 4.78 us -> 0 us
    all_gather x1 -> x0, waiting for transfers between devices: 130 us -> none  [gather_packed(): lines, at, done = (lax.all_gather(flat, axis), 0, [])]
    unnamed x3 -> x0, waiting for transfers between devices: 123 us -> none
    pallas_call x0 -> x2, Pallas kernels: none -> 75.8 us  [the longest x1 67.8 us: per_device(): pl.pallas_call(exchange_kernel, name='exchange', out_shape=(jax.ShapeDtyp...]
    all_gather x4 -> x0, blocking collectives: 59.4 us -> none  [stacked_from(): parts = lax.all_gather(parts, axes[k])]
    all_to_all x3 -> x0, starting transfers between devices: 52.1 us -> none  [sent_to_all(): return lax.all_to_all(copies, axis, split_axis=0, concat_axis=0, tiled=True)]
    all_to_all x3 -> x0, waiting for transfers between devices: 33.7 us -> none  [sent_to_all(): return lax.all_to_all(copies, axis, split_axis=0, concat_axis=0, tiled=True)]
    unnamed x1 -> x0, blocking collectives: 13.3 us -> none
    all_gather x1 -> x0, local copies, waits for them, and re-layouts: 7.37 us -> none  [gather_packed(): lines, at, done = (lax.all_gather(flat, axis), 0, [])]
  transfers between devices with their start and end apart: 5 -> 0, of which waited for: 5 -> 0; matrix products, arithmetic and copies ran while one was open for 1% -> 0% of each run, Pallas kernels for 0% -> 0%
where the time goes in v1:
time: 76.6 us; the launch traced here: 76.5 us
  Pallas kernels  75.8 us (99%)
    pallas_call x1, Pallas kernels, per_device(): pl.pallas_call(exchange_kernel, name='exchange', out_shape=(jax.ShapeDtyp...  67.8 us
    pallas_call x1, Pallas kernels, per_device(): pl.pallas_call(update_kernel, name='update', out_shape=(like((VROWS, VC))...  8.03 us

profile of v1, /device:TPU:1, one launch (start us, length us, event | category | flops | bytes accessed | tf_op | source)
XLA Modules:
  0.0 76.5 jit_solution(5743432559400491342)
XLA Ops:
  0.6 67.8 %exchange.1 = (bf16[16,4,128,256]{3,2,1,0:T(8,128)(2,1)}, bf16[4,32,768]{2,1,0:T(8,128)(2,1)}, f32[8,128]{1,0:T(8,128)}) custom-call(bf16[512,512]{1,0:T(8,128)(2,1)} %n_in.1, bf16[512,256]{1,0:T(8,128)(2,1)} %vc_in.1, bf16[512,256]{1,0:T(8,128)(2,1)} %mo_in.1, bf16[512,512]{1,0:T(8,128)(2,1)} %oc_in.1, bf16[4096,128]{1,0:T(8,128)(2,1)} %fv_in.3, ...), custom_call_target="tpu_custom_call" | custom-call | tf_op jit(solution)/shard_map/exchange/pallas_call | solution.py:441
  68.4 8.0 %update.1 = (f32[64,256]{1,0:T(8,128)}, f32[64,256]{1,0:T(8,128)}, bf16[4096,256]{1,0:T(8,128)(2,1)}, f32[128,256]{1,0:T(8,128)}, f32[128,256]{1,0:T(8,128)}, /*...) custom-call(bf16[16,4,128,256]{3,2,1,0:T(8,128)(2,1)} %get-tuple-ele, ...), custom_call_target="tpu_custom_call" | custom-call | tf_op jit(solution)/shard_map/update/pallas_call | solution.py:479

commit v2 on v1

v2 whole, which is shorter than its diff:
```python
import jax
import jax.numpy as jnp
from jax import lax
from jax.experimental import pallas as pl
from jax.experimental.pallas import tpu as pltpu
from jax.sharding import Mesh
from jax.sharding import PartitionSpec as P

D = 4096
WIDTH = 2048
R = 128
TOK = 512
NZ, NY, NT = 16, 4, 8
FEAT = D // NT
HEAD = WIDTH // NT
VC = WIDTH // NT
OC = D // NT
PC = VC + OC
VROWS = D // (NZ * NY)
OROWS = WIDTH // (NZ * NY)
BLK = VROWS + 2 * OROWS
ASPLIT = 48
BHALF = 96

BETA_ONE = 0.8
BETA_TWO = 0.9
EPSILON = 1e-08
STEP_RATE = 0.005
FLOOR = 0.25

BF = jnp.bfloat16
F32 = jnp.float32
MESH = pl.DeviceIdType.MESH


def moments(first, second, projected):
    first_new = BETA_ONE * first + (1.0 - BETA_ONE) * projected
    second_new = BETA_TWO * second + (1.0 - BETA_TWO) * projected * projected
    normalized = first_new / (jnp.sqrt(second_new) + EPSILON)
    return first_new, second_new, normalized


def exchange_kernel(
    n_in, vc_in, mo_in, oc_in, fv_in, fo_in, vw_in, vm_in, vs_in, ow_in, om_in, os_in,
    g, scales, vn_out, on_out, vmb, vsb, omb, osb, fv_all, fo_all, vwb, owb,
    nb, vcb, mob, ocb, fvb, fob,
    xs, xr, xg, pfv, pfo, pbv, pbo, yrv, yro, zs, zb, zr, zg, nat, yg, st, sr, sy, syr,
    lsem, tok,
    xs_s, xs_r, xg_s, xg_r, sc_s, sc_r, sy_s, sy_r, yr_s, yr_r, yg_s, yg_r,
    zr_s, zr_r, zg_s, zg_r, ay_s, ay_r, az_s, az_r, bz_s, bz_r, by_s, by_r,
):
    z, y, t = lax.axis_index("z"), lax.axis_index("y"), lax.axis_index("tp")

    def around(k, i, n):
        return lax.rem(k + (i + n), n)

    up, down = around(z, 1, NZ), around(z, -1, NZ)
    yup, ydown = around(y, 1, NY), around(y, -1, NY)

    barrier = pltpu.get_barrier_semaphore()
    for i in range(1, NT):
        pl.semaphore_signal(barrier, inc=1, device_id={"tp": around(t, i, NT)}, device_id_type=MESH)
    for i in range(1, NY):
        pl.semaphore_signal(barrier, inc=1, device_id={"y": around(y, i, NY)}, device_id_type=MESH)
    for k in (up, down):
        pl.semaphore_signal(barrier, inc=1, device_id={"z": k}, device_id_type=MESH)

    loads = []
    for k, (src, dst) in enumerate((
        (fo_in.at[pl.ds(pl.multiple_of(t * HEAD, HEAD), HEAD)], fob), (mo_in, mob),
        (fv_in.at[pl.ds(pl.multiple_of(t * FEAT, FEAT), FEAT)], fvb), (n_in, nb),
        (vw_in, vwb), (ow_in, owb),
        (oc_in, ocb), (vc_in, vcb),
        (vm_in, vmb), (vs_in, vsb), (om_in, omb), (os_in, osb),
        (fv_in, fv_all), (fo_in, fo_all),
    )):
        c = pltpu.make_async_copy(src, dst, lsem.at[k])
        c.start()
        loads.append(c)

    sent = []

    def remote(src, dst, ssem, rsem, **where):
        return pltpu.make_async_remote_copy(
            src_ref=src, dst_ref=dst, send_sem=ssem, recv_sem=rsem,
            device_id=where, device_id_type=MESH,
        )

    def send(src, dst, ssem, rsem, **where):
        c = remote(src, dst, ssem, rsem, **where)
        c.start()
        sent.append(c)

    def arrived(dst, rsem):
        remote(dst, dst, rsem, rsem, tp=t).wait_recv()

    def a_rows(k, ys=None):
        return g.at[k, :, pl.ds(0, ASPLIT), :] if ys is None else g.at[k, pl.ds(ys, NY // 2), pl.ds(0, ASPLIT), :]

    def b_rows(k, j=None, part=None):
        lo, hi = {None: (ASPLIT, BLK), 0: (ASPLIT, BHALF), 1: (BHALF, BLK)}[part]
        return g.at[k, y if j is None else j, pl.ds(lo, hi - lo), :]

    LAST = NZ // 2

    def a_begin():
        own = g.at[z, y, pl.ds(0, ASPLIT), :]
        for i in range(1, NY):
            send(own, own, ay_s.at[i], ay_r.at[i], y=around(y, i, NY))

    def a_ring(s):
        if s == 0:
            for i in range(1, NY):
                arrived(g.at[z, around(y, -i, NY), pl.ds(0, ASPLIT), :], ay_r.at[i])
        below, above = around(z, -s, NZ), around(z, s, NZ)
        if 0 < s < LAST:
            arrived(a_rows(below), az_r.at[0, s])
            arrived(a_rows(above), az_r.at[1, s])
        if s == LAST:
            arrived(a_rows(below, 0), az_r.at[0, s])
            arrived(a_rows(above, NY // 2), az_r.at[1, s])
            return
        half = s + 1 == LAST
        for d, (k, to) in enumerate(((below, up), (above, down))):
            block = a_rows(k, d * (NY // 2)) if half else a_rows(k)
            send(block, block, az_s.at[d, s + 1], az_r.at[d, s + 1], z=to)

    def b_across(k, b):
        block = b_rows(k)
        send(block, block, by_s.at[0, b], by_r.at[0, b], y=yup)
        send(block, block, by_s.at[1, b], by_r.at[1, b], y=ydown)

    def b_ids(s):
        if s == 0:
            return ((0, 0),)
        if s == LAST:
            return ((LAST, NZ - 1),)
        return ((-s, 2 * s - 1), (s, 2 * s))

    def b_ring(s):
        below, above = around(z, -s, NZ), around(z, s, NZ)
        if 0 < s < LAST:
            arrived(b_rows(below), bz_r.at[0, s])
            arrived(b_rows(above), bz_r.at[1, s])
        if s == LAST:
            arrived(b_rows(below, part=0), bz_r.at[0, s])
            arrived(b_rows(above, part=1), bz_r.at[1, s])
        else:
            half = s + 1 == LAST
            for d, (k, to) in enumerate(((below, up), (above, down))):
                block = b_rows(k, part=d) if half else b_rows(k)
                send(block, block, bz_s.at[d, s + 1], bz_r.at[d, s + 1], z=to)
        for off, b in b_ids(s):
            b_across(around(z, off, NZ), b)

    def b_forward(s):
        for off, b in b_ids(s):
            k = around(z, off, NZ)
            arrived(b_rows(k, ydown), by_r.at[0, b])
            block = b_rows(k, ydown, 0)
            send(block, block, by_s.at[2, b], by_r.at[2, b], y=yup)
            arrived(b_rows(k, yup), by_r.at[1, b])
            block = b_rows(k, yup, 1)
            send(block, block, by_s.at[3, b], by_r.at[3, b], y=ydown)

    def b_end(s):
        across = around(y, 2, NY)
        for off, b in b_ids(s):
            k = around(z, off, NZ)
            arrived(b_rows(k, across, 0), by_r.at[2, b])
            arrived(b_rows(k, across, 1), by_r.at[3, b])

    def token():
        pl.semaphore_signal(tok.at[0], inc=1, device_id={"z": up}, device_id_type=MESH)
        pl.semaphore_signal(tok.at[1], inc=1, device_id={"z": down}, device_id_type=MESH)
        pl.semaphore_wait(tok.at[0], 1)
        pl.semaphore_wait(tok.at[1], 1)

    nt = (((1,), (1,)), ((), ()))

    def c_partial(w):
        for c in loads[2 - 2 * w:4 - 2 * w]:
            c.wait()
        factor, rows = (fob, mob) if w else (fvb, nb)
        part = lax.dot_general(factor[...].T, rows[...], nt, preferred_element_type=F32)
        xs[w] = part.astype(BF).reshape(NT, 16, TOK)

    def c_scatter(w):
        for i in range(1, NT):
            to = around(t, i, NT)
            send(xs.at[w, to], xr.at[w, i], xs_s.at[w, i], xs_r.at[w, i], tp=to)

    def c_gather(w):
        for i in range(1, NT):
            arrived(xr.at[w, i], xs_r.at[w, i])
        total = xs[w, t].astype(F32)
        for i in range(1, NT):
            total = total + xr[w, i].astype(F32)
        xg[w, t] = total.astype(BF)
        for i in range(1, NT):
            send(xg.at[w, t], xg.at[w, t], xg_s.at[w, i], xg_r.at[w, i], tp=around(t, i, NT))

    def c_project(w):
        loads[7 - w].wait()
        for i in range(1, NT):
            arrived(xg.at[w, around(t, -i, NT)], xg_r.at[w, i])
        right, whole, rounded, landing = (ocb, pfo, pbo, yro) if w else (vcb, pfv, pbv, yrv)
        p = jnp.dot(xg[w].reshape(R, TOK), right[...], preferred_element_type=F32)
        p = p.reshape(NY, R // NY, p.shape[-1])
        whole[...] = p
        rounded[...] = p.astype(BF)
        for i in range(1, NY):
            to = around(y, i, NY)
            send(rounded.at[to], landing.at[i], yr_s.at[w, i], yr_r.at[w, i], y=to)

    def c_zscatter():
        for i in range(1, NY):
            arrived(yro.at[i], yr_r.at[1, i])
        total = pfo[y]
        for i in range(1, NY):
            total = total + yro[i].astype(F32)
        for k in range(NZ):
            q, r = divmod(k, 4)
            zs[k, 0:8, :] = total[8 * q:8 * q + 8, 128 * r:128 * r + 128]
        for i in range(1, NY):
            arrived(yrv.at[i], yr_r.at[0, i])
        total = pfv[y]
        for i in range(1, NY):
            total = total + yrv[i].astype(F32)
        for k in range(NZ):
            q, r = divmod(k, 2)
            zs[k, 8:12, :] = total[4 * q:4 * q + 4, 128 * r:128 * r + 128]
            zs[k, 12:16, :] = jnp.zeros((4, 128), F32)
        zb[...] = zs[...].astype(BF)
        for i in range(1, NZ):
            to = around(z, i, NZ)
            send(zb.at[to], zr.at[i], zr_s.at[i], zr_r.at[i], z=to)

    def c_zgather():
        for c in loads[8:12]:
            c.wait()
        down8 = pl.multiple_of(y * (R // NY) + 8 * (z // 4), 8)
        o_cols = pl.ds(pl.multiple_of(128 * lax.rem(z, 4), 128), 128)
        v_cols = pl.ds(pl.multiple_of(128 * lax.rem(z, 2), 128), 128)
        rows8 = pl.ds(down8, 8)
        om, osq = omb[rows8, o_cols], osb[rows8, o_cols]
        vm, vsq = vmb[rows8, v_cols], vsb[rows8, v_cols]
        second = lax.rem(z // 2, 2) == 1
        vm = jnp.where(second, vm[4:8], vm[0:4])
        vsq = jnp.where(second, vsq[4:8], vsq[0:4])
        for i in range(1, NZ):
            arrived(zr.at[i], zr_r.at[i])
        total = zs[z]
        for i in range(1, NZ):
            total = total + zr[i].astype(F32)
        held = total.astype(BF).astype(F32)
        _, _, on = moments(om, osq, held[0:8])
        _, _, vn = moments(vm, vsq, held[8:12])
        o_sum = jnp.sum(on * on, axis=0, keepdims=True)
        v_sum = jnp.sum(vn * vn, axis=0, keepdims=True)
        o_high, v_high = o_sum.astype(BF).astype(F32), v_sum.astype(BF).astype(F32)
        row = lax.broadcasted_iota(jnp.int32, (16, 128), 0)
        for k, line in enumerate((v_high, v_sum - v_high, o_high, o_sum - o_high)):
            total = jnp.where(row == 12 + k, line, total)
        zg[z] = total.astype(BF)
        for i in range(1, NZ):
            send(zg.at[z], zg.at[z], zg_s.at[i], zg_r.at[i], z=around(z, i, NZ))

    def c_ygather():
        for i in range(1, NZ):
            arrived(zg.at[around(z, -i, NZ)], zg_r.at[i])
        lines = jnp.zeros((4, 128), F32)
        for k in range(NZ):
            chunk = zg[k].astype(F32)
            q, r = divmod(k, 4)
            nat[8 * q:8 * q + 8, VC + 128 * r:VC + 128 * r + 128] = chunk[0:8]
            q, r = divmod(k, 2)
            nat[4 * q:4 * q + 4, 128 * r:128 * r + 128] = chunk[8:12]
            lines = lines + chunk[12:16]
        yg[y] = nat[...].astype(BF)
        for i in range(1, NY):
            send(yg.at[y], yg.at[y], yg_s.at[i], yg_r.at[i], y=around(y, i, NY))
        row = lax.broadcasted_iota(jnp.int32, (8, 128), 0)
        st[...] = jnp.where(row < 4, lines[0:1] + lines[1:2], lines[2:3] + lines[3:4])
        for i in range(1, NT):
            send(st, sr.at[i], sc_s.at[i], sc_r.at[i], tp=around(t, i, NT))

    def c_squares():
        for i in range(1, NT):
            arrived(sr.at[i], sc_r.at[i])
        total = st[...]
        for i in range(1, NT):
            total = total + sr[i]
        sy[...] = total
        for i in range(1, NY):
            send(sy, syr.at[i], sy_s.at[i], sy_r.at[i], y=around(y, i, NY))

    def c_moments():
        for i in range(1, NY):
            arrived(yg.at[around(y, -i, NY)], yg_r.at[i])
        whole = yg[...].reshape(R, PC).astype(F32)
        vmb[...], vsb[...], vn_out[...] = moments(vmb[...], vsb[...], whole[:, 0:VC])
        omb[...], osb[...], on_out[...] = moments(omb[...], osb[...], whole[:, VC:PC])

    def c_scales():
        for i in range(1, NY):
            arrived(syr.at[i], sy_r.at[i])
        total = sy[...]
        for i in range(1, NY):
            total = total + syr[i]
        row = lax.broadcasted_iota(jnp.int32, (8, 128), 0)
        mean = jnp.sum(total, axis=1, keepdims=True) * jnp.where(row < 4, 1.0 / (R * WIDTH), 1.0 / (R * D))
        scales[...] = lax.rsqrt(mean + FLOOR)

    c_partial(1)
    pl.semaphore_wait(barrier, NT + NY)
    c_scatter(1)
    c_partial(0)
    c_scatter(0)
    for c in loads[4:6]:
        c.wait()
    g[z, y, 0:VROWS, :] = vwb[...].astype(BF)
    g[z, y, VROWS:VROWS + OROWS, :] = owb[:, 0:VC].astype(BF)
    g[z, y, VROWS + OROWS:BLK, :] = owb[:, VC:OC].astype(BF)
    a_begin()
    b_ring(0)
    token()
    token()
    c_gather(1)
    token()
    a_ring(0)
    c_gather(0)
    token()
    token()
    b_ring(1)
    b_forward(0)
    c_project(1)
    c_project(0)
    token()
    token()
    a_ring(1)
    b_ring(2)
    b_forward(1)
    c_zscatter()
    a_ring(2)
    b_ring(3)
    b_forward(2)
    a_ring(3)
    b_ring(4)
    b_forward(3)
    c_zgather()
    a_ring(4)
    b_ring(5)
    b_forward(4)
    a_ring(5)
    b_ring(6)
    b_forward(5)
    c_ygather()
    a_ring(6)
    b_ring(7)
    b_forward(6)
    c_squares()
    a_ring(7)
    b_ring(8)
    b_forward(7)
    c_moments()
    b_forward(8)
    c_scales()
    a_ring(8)
    for s in range(LAST + 1):
        b_end(s)
    for c in loads[12:]:
        c.wait()
    for c in sent:
        c.wait_send()


def update_kernel(
    g, scales, vn, on, vm, vs, om, os, fv, fo, vw, ow,
    vstep_out, vnew_out, vcopy_out, vm_out, vs_out, ostep_out, onew_out, ocopy_out, om_out, os_out,
    vstep, vnew, vcopy, ostep, onew, ocopy, wsem, vcsem, ocsem,
):
    z, y = lax.axis_index("z"), lax.axis_index("y")
    row = z * NY + y
    writes = []

    def write(src, dst, sem):
        c = pltpu.make_async_copy(src, dst, sem)
        c.start()
        writes.append(c)

    for k, (src, dst) in enumerate(((vm, vm_out), (vs, vs_out), (om, om_out), (os, os_out))):
        write(src, dst, wsem.at[k])
    v_scale = scales[0:1, 0:1]
    o_scale = scales[4:5, 0:1]

    def two(normalized, scale):
        scaled = normalized * (scale * STEP_RATE)
        high = scaled.astype(BF)
        low = (scaled - high.astype(F32)).astype(BF)
        return jnp.concatenate([high, low], axis=0)

    v_two = two(vn[...], v_scale)
    o_two = two(on[...], o_scale)
    vt, ot = NY * VROWS, NY * OROWS
    for k in range(NZ):
        f = fv[k * vt:(k + 1) * vt, :]
        delta = jnp.dot(jnp.concatenate([f, f], axis=1), v_two, preferred_element_type=F32)
        held = g[k, :, 0:VROWS, :].reshape(vt, VC).astype(F32)
        vcopy[k * vt:(k + 1) * vt, :] = (held - delta).astype(BF)
        write(vcopy.at[pl.ds(k * vt, vt)], vcopy_out.at[pl.ds(k * vt, vt)], vcsem.at[k])
        f = fo[k * ot:(k + 1) * ot, :]
        delta = jnp.dot(jnp.concatenate([f, f], axis=1), o_two, preferred_element_type=F32)
        for h in range(2):
            lo = VROWS + h * OROWS
            held = g[k, :, lo:lo + OROWS, :].reshape(ot, VC).astype(F32)
            ocopy[k * ot:(k + 1) * ot, h * VC:(h + 1) * VC] = (held - delta[:, h * VC:(h + 1) * VC]).astype(BF)
        write(ocopy.at[pl.ds(k * ot, ot)], ocopy_out.at[pl.ds(k * ot, ot)], ocsem.at[k])
    highest = lax.Precision.HIGHEST
    v_here = fv[pl.ds(pl.multiple_of(row * VROWS, VROWS), VROWS), :].astype(F32)
    o_here = fo[pl.ds(pl.multiple_of(row * OROWS, OROWS), OROWS), :].astype(F32)
    vstep[...] = v_scale * jnp.dot(v_here, vn[...], precision=highest, preferred_element_type=F32)
    ostep[...] = o_scale * jnp.dot(o_here, on[...], precision=highest, preferred_element_type=F32)
    vnew[...] = vw[...] - STEP_RATE * vstep[...]
    onew[...] = ow[...] - STEP_RATE * ostep[...]
    for k, (src, dst) in enumerate(((vstep, vstep_out), (vnew, vnew_out), (ostep, ostep_out), (onew, onew_out))):
        write(src, dst, wsem.at[4 + k])
    for c in writes:
        c.wait()


def per_device(
    normed_input, value_cotangent, mixer_output, output_cotangent, value_factor, output_factor,
    value_master, value_moment, value_second, output_master, output_moment, output_second,
):
    anywhere = pl.BlockSpec(memory_space=pl.ANY)
    inside = pl.BlockSpec(memory_space=pltpu.VMEM)
    dma = pltpu.SemaphoreType.DMA

    def vmem(shape, dtype):
        return pltpu.VMEM(shape, dtype)

    handed = (
        vmem((NZ, NY, BLK, VC), BF), vmem((8, 128), F32), vmem((R, VC), F32), vmem((R, OC), F32),
        vmem((R, VC), F32), vmem((R, VC), F32), vmem((R, OC), F32), vmem((R, OC), F32),
        vmem((D, R), BF), vmem((WIDTH, R), BF), vmem((VROWS, VC), F32), vmem((OROWS, OC), F32),
    )
    state = pl.pallas_call(
        exchange_kernel,
        name="exchange",
        out_shape=handed,
        in_specs=[anywhere] * 12,
        out_specs=(inside,) * len(handed),
        scratch_shapes=[
            vmem((TOK, FEAT), BF), vmem((TOK, VC), BF), vmem((TOK, HEAD), BF), vmem((TOK, OC), BF),
            vmem((FEAT, R), BF), vmem((HEAD, R), BF),
            vmem((2, NT, 16, TOK), BF), vmem((2, NT, 16, TOK), BF), vmem((2, NT, 16, TOK), BF),
            vmem((NY, R // NY, VC), F32), vmem((NY, R // NY, OC), F32),
            vmem((NY, R // NY, VC), BF), vmem((NY, R // NY, OC), BF),
            vmem((NY, R // NY, VC), BF), vmem((NY, R // NY, OC), BF),
            vmem((NZ, 16, 128), F32), vmem((NZ, 16, 128), BF), vmem((NZ, 16, 128), BF), vmem((NZ, 16, 128), BF),
            vmem((R // NY, PC), F32), vmem((NY, R // NY, PC), BF),
            vmem((8, 128), F32), vmem((NT, 8, 128), F32), vmem((8, 128), F32), vmem((NY, 8, 128), F32),
            dma((14,)), pltpu.SemaphoreType.REGULAR((2,)),
            dma((2, NT)), dma((2, NT)), dma((2, NT)), dma((2, NT)), dma((NT,)), dma((NT,)), dma((NY,)), dma((NY,)),
            dma((2, NY)), dma((2, NY)), dma((NY,)), dma((NY,)),
            dma((NZ,)), dma((NZ,)), dma((NZ,)), dma((NZ,)),
            dma((NY,)), dma((NY,)),
            dma((2, NZ // 2 + 1)), dma((2, NZ // 2 + 1)), dma((2, NZ // 2 + 1)), dma((2, NZ // 2 + 1)),
            dma((4, NZ)), dma((4, NZ)),
        ],
        compiler_params=pltpu.CompilerParams(collective_id=0, has_side_effects=True, vmem_limit_bytes=30 << 20),
    )(
        normed_input, value_cotangent, mixer_output, output_cotangent, value_factor, output_factor,
        value_master, value_moment, value_second, output_master, output_moment, output_second,
    )

    def like(a, dtype=F32):
        return jax.ShapeDtypeStruct(a, dtype)

    return pl.pallas_call(
        update_kernel,
        name="update",
        out_shape=(
            like((VROWS, VC)), like((VROWS, VC)), like((D, VC), BF), like((R, VC)), like((R, VC)),
            like((OROWS, OC)), like((OROWS, OC)), like((WIDTH, OC), BF), like((R, OC)), like((R, OC)),
        ),
        in_specs=[inside] * len(handed),
        out_specs=(anywhere,) * 10,
        scratch_shapes=[
            vmem((VROWS, VC), F32), vmem((VROWS, VC), F32), vmem((D, VC), BF),
            vmem((OROWS, OC), F32), vmem((OROWS, OC), F32), vmem((WIDTH, OC), BF),
            dma((8,)), dma((NZ,)), dma((NZ,)),
        ],
        compiler_params=pltpu.CompilerParams(vmem_limit_bytes=30 << 20),
    )(*state)


def solution(mesh):
    finer = Mesh(mesh.devices.reshape(NZ, NY, NT), ("z", "y", "tp"))
    fs = ("z", "y")
    rows, cols = P(fs, "tp"), P(None, "tp")
    return jax.shard_map(
        per_device,
        mesh=finer,
        in_specs=(rows, rows, rows, rows, P(), P(), rows, cols, cols, rows, cols, cols),
        out_specs=(rows, rows, cols, cols, cols, rows, rows, cols, cols, cols),
        check_vma=False,
    )
```

time: 76.6 us -> 81.9 us (1.069)
  the two profiles are of different devices: /device:TPU:1 before, /device:TPU:8 now
where the time goes in v2:
time: 81.9 us; the launch traced here: 81.3 us
  Pallas kernels  69 us (84%)
  local copies, waits for them, and re-layouts  11.6 us (14%)
    pallas_call x1, Pallas kernels, per_device(): pl.pallas_call(exchange_kernel, name='exchange', out_shape=handed, in_spe...  66.1 us
    unnamed x24, local copies, waits for them, and re-layouts  11.6 us
    pallas_call x1, Pallas kernels, per_device(): pl.pallas_call(update_kernel, name='update', out_shape=(like((VROWS, VC))...  2.95 us

profile of v2, /device:TPU:8, one launch (start us, length us, event | category | flops | bytes accessed | tf_op | source)
XLA Modules:
  0.0 81.3 jit_solution(8846231188616000005)
XLA Ops:
  0.6 0.0 copy-start
  0.7 1.2 %copy-done = bf16[4096,128]{1,0:T(8,128)(2,1)S(1)} copy-done((bf16[4096,128]{1,0:T(8,128)(2,1)S(1)}, bf16[4096,128]{1,0:T(8,128)(2,1)}, u32[]{:S(2)}) %copy-start) | copy-done | bytes 1048600
  1.9 0.0 copy-start.1
  1.9 1.0 %copy-done.1 = bf16[512,512]{1,0:T(8,128)(2,1)S(1)} copy-done((bf16[512,512]{1,0:T(8,128)(2,1)S(1)}, bf16[512,512]{1,0:T(8,128)(2,1)}, u32[]{:S(2)}) %copy-start.1) | copy-done | bytes 524312
  2.9 0.0 copy-start.2
  2.9 1.0 %copy-done.2 = bf16[512,512]{1,0:T(8,128)(2,1)S(1)} copy-done((bf16[512,512]{1,0:T(8,128)(2,1)S(1)}, bf16[512,512]{1,0:T(8,128)(2,1)}, u32[]{:S(2)}) %copy-start.2) | copy-done | bytes 524312
  4.0 0.0 copy-start.3
  4.0 1.0 %copy-done.3 = bf16[2048,128]{1,0:T(8,128)(2,1)S(1)} copy-done((bf16[2048,128]{1,0:T(8,128)(2,1)S(1)}, bf16[2048,128]{1,0:T(8,128)(2,1)}, u32[]{:S(2)}) %copy-start.3) | copy-done | bytes 524312
  5.0 0.0 copy-start.4
  5.0 0.9 %copy-done.4 = bf16[512,256]{1,0:T(8,128)(2,1)S(1)} copy-done((bf16[512,256]{1,0:T(8,128)(2,1)S(1)}, bf16[512,256]{1,0:T(8,128)(2,1)}, u32[]{:S(2)}) %copy-start.4) | copy-done | bytes 262168
  6.0 0.0 copy-start.5
  6.0 0.9 %copy-done.5 = bf16[512,256]{1,0:T(8,128)(2,1)S(1)} copy-done((bf16[512,256]{1,0:T(8,128)(2,1)S(1)}, bf16[512,256]{1,0:T(8,128)(2,1)}, u32[]{:S(2)}) %copy-start.5) | copy-done | bytes 262168
  6.9 0.0 copy-start.6
  6.9 0.9 %copy-done.6 = f32[128,512]{1,0:T(8,128)S(1)} copy-done((f32[128,512]{1,0:T(8,128)S(1)}, f32[128,512]{1,0:T(8,128)}, u32[]{:S(2)}) %copy-start.6) | copy-done | bytes 262168
  7.9 0.0 copy-start.7
  7.9 0.9 %copy-done.7 = f32[128,512]{1,0:T(8,128)S(1)} copy-done((f32[128,512]{1,0:T(8,128)S(1)}, f32[128,512]{1,0:T(8,128)}, u32[]{:S(2)}) %copy-start.7) | copy-done | bytes 262168
  8.8 0.0 copy-start.8
  8.8 0.9 %copy-done.8 = f32[128,256]{1,0:T(8,128)S(1)} copy-done((f32[128,256]{1,0:T(8,128)S(1)}, f32[128,256]{1,0:T(8,128)}, u32[]{:S(2)}) %copy-start.8) | copy-done | bytes 131096
  9.7 0.0 copy-start.9
  9.7 0.9 %copy-done.9 = f32[128,256]{1,0:T(8,128)S(1)} copy-done((f32[128,256]{1,0:T(8,128)S(1)}, f32[128,256]{1,0:T(8,128)}, u32[]{:S(2)}) %copy-start.9) | copy-done | bytes 131096
  10.6 0.0 copy-start.10
  10.6 0.8 %copy-done.10 = f32[64,256]{1,0:T(8,128)S(1)} copy-done((f32[64,256]{1,0:T(8,128)S(1)}, f32[64,256]{1,0:T(8,128)}, u32[]{:S(2)}) %copy-start.10) | copy-done | bytes 65560
  11.5 0.0 copy-start.11
  11.5 0.8 %copy-done.11 = f32[32,512]{1,0:T(8,128)S(1)} copy-done((f32[32,512]{1,0:T(8,128)S(1)}, f32[32,512]{1,0:T(8,128)}, u32[]{:S(2)}) %copy-start.11) | copy-done | bytes 65560
  12.3 66.1 %exchange.1 = (bf16[16,4,128,256]{3,2,1,0:T(8,128)(2,1)S(1)}, f32[8,128]{1,0:T(8,128)S(1)}, f32[128,256]{1,0:T(8,128)S(1)}, f32[128,512]{1,0:T(8,128)S(1)}, f32[...) custom-call(bf16[512,512]{1,0:T(8,128)(2,1)S(1)} %copy-done.1, ...), custom_call_target="tpu_custom_call" | custom-call | tf_op jit(solution)/shard_map/exchange/pallas_call | solution.py:448
  78.4 3.0 %update.1 = (f32[64,256]{1,0:T(8,128)}, f32[64,256]{1,0:T(8,128)}, bf16[4096,256]{1,0:T(8,128)(2,1)}, f32[128,256]{1,0:T(8,128)}, f32[128,256]{1,0:T(8,128)}, /*...) custom-call(bf16[16,4,128,256]{3,2,1,0:T(8,128)(2,1)S(1)} %get-tuple, ...), custom_call_target="tpu_custom_call" | custom-call | tf_op jit(solution)/shard_map/update/pallas_call | solution.py:481
Async XLA Ops:
  0.6 1.2 %copy-start = (bf16[4096,128]{1,0:T(8,128)(2,1)S(1)}, bf16[4096,128]{1,0:T(8,128)(2,1)}, u32[]{:S(2)}) copy-start(bf16[4096,128]{1,0:T(8,128)(2,1)} %fv_in.1) | copy-start | bytes 3145732
  1.9 1.0 %copy-start.1 = (bf16[512,512]{1,0:T(8,128)(2,1)S(1)}, bf16[512,512]{1,0:T(8,128)(2,1)}, u32[]{:S(2)}) copy-start(bf16[512,512]{1,0:T(8,128)(2,1)} %n_in.1) | copy-start | bytes 1572868
  2.9 1.0 %copy-start.2 = (bf16[512,512]{1,0:T(8,128)(2,1)S(1)}, bf16[512,512]{1,0:T(8,128)(2,1)}, u32[]{:S(2)}) copy-start(bf16[512,512]{1,0:T(8,128)(2,1)} %oc_in.1) | copy-start | bytes 1572868
  4.0 1.0 %copy-start.3 = (bf16[2048,128]{1,0:T(8,128)(2,1)S(1)}, bf16[2048,128]{1,0:T(8,128)(2,1)}, u32[]{:S(2)}) copy-start(bf16[2048,128]{1,0:T(8,128)(2,1)} %fo_in.1) | copy-start | bytes 1572868
  5.0 0.9 %copy-start.4 = (bf16[512,256]{1,0:T(8,128)(2,1)S(1)}, bf16[512,256]{1,0:T(8,128)(2,1)}, u32[]{:S(2)}) copy-start(bf16[512,256]{1,0:T(8,128)(2,1)} %vc_in.1) | copy-start | bytes 786436
  6.0 0.9 %copy-start.5 = (bf16[512,256]{1,0:T(8,128)(2,1)S(1)}, bf16[512,256]{1,0:T(8,128)(2,1)}, u32[]{:S(2)}) copy-start(bf16[512,256]{1,0:T(8,128)(2,1)} %mo_in.1) | copy-start | bytes 786436
  6.9 0.9 %copy-start.6 = (f32[128,512]{1,0:T(8,128)S(1)}, f32[128,512]{1,0:T(8,128)}, u32[]{:S(2)}) copy-start(f32[128,512]{1,0:T(8,128)} %om_in.1) | copy-start | bytes 786436
  7.9 0.9 %copy-start.7 = (f32[128,512]{1,0:T(8,128)S(1)}, f32[128,512]{1,0:T(8,128)}, u32[]{:S(2)}) copy-start(f32[128,512]{1,0:T(8,128)} %os_in.1) | copy-start | bytes 786436
  8.8 0.9 %copy-start.8 = (f32[128,256]{1,0:T(8,128)S(1)}, f32[128,256]{1,0:T(8,128)}, u32[]{:S(2)}) copy-start(f32[128,256]{1,0:T(8,128)} %vm_in.1) | copy-start | bytes 393220
  9.7 0.9 %copy-start.9 = (f32[128,256]{1,0:T(8,128)S(1)}, f32[128,256]{1,0:T(8,128)}, u32[]{:S(2)}) copy-start(f32[128,256]{1,0:T(8,128)} %vs_in.1) | copy-start | bytes 393220
  10.6 0.8 %copy-start.10 = (f32[64,256]{1,0:T(8,128)S(1)}, f32[64,256]{1,0:T(8,128)}, u32[]{:S(2)}) copy-start(f32[64,256]{1,0:T(8,128)} %vw_in.1) | copy-start | bytes 196612
  11.5 0.8 %copy-start.11 = (f32[32,512]{1,0:T(8,128)S(1)}, f32[32,512]{1,0:T(8,128)}, u32[]{:S(2)}) copy-start(f32[32,512]{1,0:T(8,128)} %ow_in.1) | copy-start | bytes 196612

commit v3 on v2

--- a/solution.py
+++ b/solution.py
@@ -19,8 +19,8 @@
 VROWS = D // (NZ * NY)
 OROWS = WIDTH // (NZ * NY)
 BLK = VROWS + 2 * OROWS
-ASPLIT = 48
-BHALF = 96
+ASPLIT = 16
+BHALF = 64
 
 BETA_ONE = 0.8
 BETA_TWO = 0.9
@@ -67,9 +67,9 @@
 
     loads = []
     for k, (src, dst) in enumerate((
+        (vw_in, vwb), (ow_in, owb),
         (fo_in.at[pl.ds(pl.multiple_of(t * HEAD, HEAD), HEAD)], fob), (mo_in, mob),
         (fv_in.at[pl.ds(pl.multiple_of(t * FEAT, FEAT), FEAT)], fvb), (n_in, nb),
-        (vw_in, vwb), (ow_in, owb),
         (oc_in, ocb), (vc_in, vcb),
         (vm_in, vmb), (vs_in, vsb), (om_in, omb), (os_in, osb),
         (fv_in, fv_all), (fo_in, fo_all),
@@ -94,8 +94,8 @@
     def arrived(dst, rsem):
         remote(dst, dst, rsem, rsem, tp=t).wait_recv()
 
-    def a_rows(k, ys=None):
-        return g.at[k, :, pl.ds(0, ASPLIT), :] if ys is None else g.at[k, pl.ds(ys, NY // 2), pl.ds(0, ASPLIT), :]
+    def a_rows(k, h):
+        return g.at[k, pl.ds(h * (NY // 2), NY // 2), pl.ds(0, ASPLIT), :]
 
     def b_rows(k, j=None, part=None):
         lo, hi = {None: (ASPLIT, BLK), 0: (ASPLIT, BHALF), 1: (BHALF, BLK)}[part]
@@ -108,22 +108,15 @@
         for i in range(1, NY):
             send(own, own, ay_s.at[i], ay_r.at[i], y=around(y, i, NY))
 
-    def a_ring(s):
-        if s == 0:
+    def a_ring(s, h):
+        if s == 0 and h == 0:
             for i in range(1, NY):
                 arrived(g.at[z, around(y, -i, NY), pl.ds(0, ASPLIT), :], ay_r.at[i])
-        below, above = around(z, -s, NZ), around(z, s, NZ)
-        if 0 < s < LAST:
-            arrived(a_rows(below), az_r.at[0, s])
-            arrived(a_rows(above), az_r.at[1, s])
-        if s == LAST:
-            arrived(a_rows(below, 0), az_r.at[0, s])
-            arrived(a_rows(above, NY // 2), az_r.at[1, s])
-            return
-        half = s + 1 == LAST
-        for d, (k, to) in enumerate(((below, up), (above, down))):
-            block = a_rows(k, d * (NY // 2)) if half else a_rows(k)
-            send(block, block, az_s.at[d, s + 1], az_r.at[d, s + 1], z=to)
+        for d, (k, to) in enumerate(((around(z, -s, NZ), up), (around(z, s, NZ), down))):
+            if 0 < s < LAST or (s == LAST and d == h):
+                arrived(a_rows(k, h), az_r.at[d, h, s])
+            if s + 1 < LAST or (s + 1 == LAST and d == h):
+                send(a_rows(k, h), a_rows(k, h), az_s.at[d, h, s + 1], az_r.at[d, h, s + 1], z=to)
 
     def b_across(k, b):
         block = b_rows(k)
@@ -179,7 +172,7 @@
     nt = (((1,), (1,)), ((), ()))
 
     def c_partial(w):
-        for c in loads[2 - 2 * w:4 - 2 * w]:
+        for c in loads[4 - 2 * w:6 - 2 * w]:
             c.wait()
         factor, rows = (fob, mob) if w else (fvb, nb)
         part = lax.dot_general(factor[...].T, rows[...], nt, preferred_element_type=F32)
@@ -312,61 +305,70 @@
         mean = jnp.sum(total, axis=1, keepdims=True) * jnp.where(row < 4, 1.0 / (R * WIDTH), 1.0 / (R * D))
         scales[...] = lax.rsqrt(mean + FLOOR)
 
-    c_partial(1)
-    pl.semaphore_wait(barrier, NT + NY)
-    c_scatter(1)
-    c_partial(0)
-    c_scatter(0)
-    for c in loads[4:6]:
+    for c in loads[0:2]:
         c.wait()
     g[z, y, 0:VROWS, :] = vwb[...].astype(BF)
     g[z, y, VROWS:VROWS + OROWS, :] = owb[:, 0:VC].astype(BF)
     g[z, y, VROWS + OROWS:BLK, :] = owb[:, VC:OC].astype(BF)
+    pl.semaphore_wait(barrier, NT + NY)
     a_begin()
     b_ring(0)
-    token()
+    c_partial(1)
+    c_scatter(1)
+    c_partial(0)
+    c_scatter(0)
+    b_ring(1)
+    a_ring(0, 0)
+    a_ring(0, 1)
+    token()
+    token()
+    b_ring(2)
     token()
     c_gather(1)
-    token()
-    a_ring(0)
     c_gather(0)
-    token()
-    token()
-    b_ring(1)
     b_forward(0)
+    a_ring(1, 0)
+    a_ring(1, 1)
+    b_ring(3)
+    token()
+    token()
     c_project(1)
     c_project(0)
     token()
     token()
-    a_ring(1)
-    b_ring(2)
+    a_ring(2, 0)
+    a_ring(2, 1)
+    b_ring(4)
     b_forward(1)
     c_zscatter()
-    a_ring(2)
-    b_ring(3)
+    a_ring(3, 0)
+    a_ring(3, 1)
+    b_ring(5)
     b_forward(2)
-    a_ring(3)
-    b_ring(4)
+    a_ring(4, 0)
+    a_ring(4, 1)
+    b_ring(6)
     b_forward(3)
     c_zgather()
-    a_ring(4)
-    b_ring(5)
+    a_ring(5, 0)
+    a_ring(5, 1)
+    b_ring(7)
     b_forward(4)
-    a_ring(5)
-    b_ring(6)
+    a_ring(6, 0)
+    a_ring(6, 1)
+    b_ring(8)
     b_forward(5)
     c_ygather()
-    a_ring(6)
-    b_ring(7)
+    a_ring(7, 0)
+    a_ring(7, 1)
     b_forward(6)
+    b_forward(7)
     c_squares()
-    a_ring(7)
-    b_ring(8)
-    b_forward(7)
+    b_forward(8)
     c_moments()
-    b_forward(8)
     c_scales()
-    a_ring(8)
+    a_ring(8, 0)
+    a_ring(8, 1)
     for s in range(LAST + 1):
         b_end(s)
     for c in loads[12:]:
@@ -466,10 +468,10 @@
             dma((2, NY)), dma((2, NY)), dma((NY,)), dma((NY,)),
             dma((NZ,)), dma((NZ,)), dma((NZ,)), dma((NZ,)),
             dma((NY,)), dma((NY,)),
-            dma((2, NZ // 2 + 1)), dma((2, NZ // 2 + 1)), dma((2, NZ // 2 + 1)), dma((2, NZ // 2 + 1)),
+            dma((2, 2, NZ // 2 + 1)), dma((2, 2, NZ // 2 + 1)), dma((2, NZ // 2 + 1)), dma((2, NZ // 2 + 1)),
             dma((4, NZ)), dma((4, NZ)),
         ],
-        compiler_params=pltpu.CompilerParams(collective_id=0, has_side_effects=True, vmem_limit_bytes=30 << 20),
+        compiler_params=pltpu.CompilerParams(collective_id=0, has_side_effects=True, vmem_limit_bytes=59_900_000),
     )(
         normed_input, value_cotangent, mixer_output, output_cotangent, value_factor, output_factor,
         value_master, value_moment, value_second, output_master, output_moment, output_second,

time: 81.9 us -> 65 us (0.79)
  the two profiles are of different devices: /device:TPU:8 before, /device:TPU:1 now
where the time goes in v3:
time: 65 us; the launch traced here: 64.5 us
  Pallas kernels  63.9 us (98%)
  between operations  0.66 us (1%)
    pallas_call x1, Pallas kernels, per_device(): pl.pallas_call(exchange_kernel, name='exchange', out_shape=handed, in_spe...  60.9 us
    pallas_call x1, Pallas kernels, per_device(): pl.pallas_call(update_kernel, name='update', out_shape=(like((VROWS, VC))...  2.94 us

profile of v3, /device:TPU:1, one launch (start us, length us, event | category | flops | bytes accessed | tf_op | source)
XLA Modules:
  0.0 64.5 jit_solution(2446896154083686611)
XLA Ops:
  0.6 60.9 %exchange.1 = (bf16[16,4,128,256]{3,2,1,0:T(8,128)(2,1)S(1)}, f32[8,128]{1,0:T(8,128)S(1)}, f32[128,256]{1,0:T(8,128)S(1)}, f32[128,512]{1,0:T(8,128)S(1)}, f32[...) custom-call(bf16[512,512]{1,0:T(8,128)(2,1)} %n_in.1, ...), custom_call_target="tpu_custom_call" | custom-call | tf_op jit(solution)/shard_map/exchange/pallas_call | solution.py:450
  61.6 2.9 %update.1 = (f32[64,256]{1,0:T(8,128)}, f32[64,256]{1,0:T(8,128)}, bf16[4096,256]{1,0:T(8,128)(2,1)}, f32[128,256]{1,0:T(8,128)}, f32[128,256]{1,0:T(8,128)}, /*...) custom-call(bf16[16,4,128,256]{3,2,1,0:T(8,128)(2,1)S(1)} %get-tuple, ...), custom_call_target="tpu_custom_call" | custom-call | tf_op jit(solution)/shard_map/update/pallas_call | solution.py:483

commit v4 on v3

--- a/solution.py
+++ b/solution.py
@@ -21,6 +21,7 @@
 BLK = VROWS + 2 * OROWS
 ASPLIT = 16
 BHALF = 64
+REACH = 2
 
 BETA_ONE = 0.8
 BETA_TWO = 0.9
@@ -62,8 +63,9 @@
         pl.semaphore_signal(barrier, inc=1, device_id={"tp": around(t, i, NT)}, device_id_type=MESH)
     for i in range(1, NY):
         pl.semaphore_signal(barrier, inc=1, device_id={"y": around(y, i, NY)}, device_id_type=MESH)
-    for k in (up, down):
-        pl.semaphore_signal(barrier, inc=1, device_id={"z": k}, device_id_type=MESH)
+    for i in range(1, REACH + 1):
+        for k in (i, -i):
+            pl.semaphore_signal(barrier, inc=1, device_id={"z": around(z, k, NZ)}, device_id_type=MESH)
 
     loads = []
     for k, (src, dst) in enumerate((
@@ -131,18 +133,13 @@
         return ((-s, 2 * s - 1), (s, 2 * s))
 
     def b_ring(s):
-        below, above = around(z, -s, NZ), around(z, s, NZ)
-        if 0 < s < LAST:
-            arrived(b_rows(below), bz_r.at[0, s])
-            arrived(b_rows(above), bz_r.at[1, s])
-        if s == LAST:
-            arrived(b_rows(below, part=0), bz_r.at[0, s])
-            arrived(b_rows(above, part=1), bz_r.at[1, s])
-        else:
-            half = s + 1 == LAST
-            for d, (k, to) in enumerate(((below, up), (above, down))):
-                block = b_rows(k, part=d) if half else b_rows(k)
-                send(block, block, bz_s.at[d, s + 1], bz_r.at[d, s + 1], z=to)
+        for h in range(2):
+            for d, (k, to) in enumerate(((around(z, -s, NZ), up), (around(z, s, NZ), down))):
+                block = b_rows(k, part=h)
+                if 0 < s < LAST or (s == LAST and d == h):
+                    arrived(block, bz_r.at[d, h, s])
+                if s + 1 < LAST or (s + 1 == LAST and d == h):
+                    send(block, block, bz_s.at[d, h, s + 1], bz_r.at[d, h, s + 1], z=to)
         for off, b in b_ids(s):
             b_across(around(z, off, NZ), b)
 
@@ -163,11 +160,13 @@
             arrived(b_rows(k, across, 0), by_r.at[2, b])
             arrived(b_rows(k, across, 1), by_r.at[3, b])
 
-    def token():
-        pl.semaphore_signal(tok.at[0], inc=1, device_id={"z": up}, device_id_type=MESH)
-        pl.semaphore_signal(tok.at[1], inc=1, device_id={"z": down}, device_id_type=MESH)
-        pl.semaphore_wait(tok.at[0], 1)
-        pl.semaphore_wait(tok.at[1], 1)
+    def token(k):
+        if k > 0:
+            pl.semaphore_wait(tok.at[0], 1)
+            pl.semaphore_wait(tok.at[1], 1)
+        if REACH * (k + 1) < LAST:
+            for j, i in enumerate((REACH, -REACH)):
+                pl.semaphore_signal(tok.at[j], inc=1, device_id={"z": around(z, i, NZ)}, device_id_type=MESH)
 
     nt = (((1,), (1,)), ((), ()))
 
@@ -310,36 +309,33 @@
     g[z, y, 0:VROWS, :] = vwb[...].astype(BF)
     g[z, y, VROWS:VROWS + OROWS, :] = owb[:, 0:VC].astype(BF)
     g[z, y, VROWS + OROWS:BLK, :] = owb[:, VC:OC].astype(BF)
-    pl.semaphore_wait(barrier, NT + NY)
+    pl.semaphore_wait(barrier, NT + NY - 2 + 2 * REACH)
+    token(0)
     a_begin()
     b_ring(0)
     c_partial(1)
     c_scatter(1)
     c_partial(0)
     c_scatter(0)
+    token(1)
     b_ring(1)
     a_ring(0, 0)
     a_ring(0, 1)
-    token()
-    token()
+    token(2)
     b_ring(2)
-    token()
     c_gather(1)
     c_gather(0)
     b_forward(0)
     a_ring(1, 0)
     a_ring(1, 1)
     b_ring(3)
-    token()
-    token()
     c_project(1)
     c_project(0)
-    token()
-    token()
     a_ring(2, 0)
     a_ring(2, 1)
     b_ring(4)
     b_forward(1)
+    token(3)
     c_zscatter()
     a_ring(3, 0)
     a_ring(3, 1)
@@ -356,9 +352,9 @@
     b_forward(4)
     a_ring(6, 0)
     a_ring(6, 1)
-    b_ring(8)
     b_forward(5)
     c_ygather()
+    b_ring(8)
     a_ring(7, 0)
     a_ring(7, 1)
     b_forward(6)
@@ -468,7 +464,7 @@
             dma((2, NY)), dma((2, NY)), dma((NY,)), dma((NY,)),
             dma((NZ,)), dma((NZ,)), dma((NZ,)), dma((NZ,)),
             dma((NY,)), dma((NY,)),
-            dma((2, 2, NZ // 2 + 1)), dma((2, 2, NZ // 2 + 1)), dma((2, NZ // 2 + 1)), dma((2, NZ // 2 + 1)),
+            dma((2, 2, NZ // 2 + 1)), dma((2, 2, NZ // 2 + 1)), dma((2, 2, NZ // 2 + 1)), dma((2, 2, NZ // 2 + 1)),
             dma((4, NZ)), dma((4, NZ)),
         ],
         compiler_params=pltpu.CompilerParams(collective_id=0, has_side_effects=True, vmem_limit_bytes=59_900_000),

time: 65 us -> 62.5 us (0.962)
  Pallas kernels: 63.9 us -> 61.8 us
    pallas_call x1, Pallas kernels: 60.9 us -> 58.8 us  [per_device(): pl.pallas_call(exchange_kernel, name='exchange', out_shape=handed, in_spe...]
where the time goes in v4:
time: 62.5 us; the launch traced here: 62.4 us
  Pallas kernels  61.8 us (99%)
  between operations  0.66 us (1%)
    pallas_call x1, Pallas kernels, per_device(): pl.pallas_call(exchange_kernel, name='exchange', out_shape=handed, in_spe...  58.8 us
    pallas_call x1, Pallas kernels, per_device(): pl.pallas_call(update_kernel, name='update', out_shape=(like((VROWS, VC))...  2.95 us

profile of v4, /device:TPU:1, one launch (start us, length us, event | category | flops | bytes accessed | tf_op | source)
XLA Modules:
  0.0 62.4 jit_solution(517119855213300734)
XLA Ops:
  0.6 58.8 %exchange.1 = (bf16[16,4,128,256]{3,2,1,0:T(8,128)(2,1)S(1)}, f32[8,128]{1,0:T(8,128)S(1)}, f32[128,256]{1,0:T(8,128)S(1)}, f32[128,512]{1,0:T(8,128)S(1)}, f32[...) custom-call(bf16[512,512]{1,0:T(8,128)(2,1)} %n_in.1, ...), custom_call_target="tpu_custom_call" | custom-call | tf_op jit(solution)/shard_map/exchange/pallas_call | solution.py:446
  59.5 2.9 %update.1 = (f32[64,256]{1,0:T(8,128)}, f32[64,256]{1,0:T(8,128)}, bf16[4096,256]{1,0:T(8,128)(2,1)}, f32[128,256]{1,0:T(8,128)}, f32[128,256]{1,0:T(8,128)}, /*...) custom-call(bf16[16,4,128,256]{3,2,1,0:T(8,128)(2,1)S(1)} %get-tuple, ...), custom_call_target="tpu_custom_call" | custom-call | tf_op jit(solution)/shard_map/update/pallas_call | solution.py:479
